TPU v7x, 32 devices: a whole 2x2x4 slice. The times are simulated.
32 devices in a mesh: rep: 2 (over x), fs: 8 (over z, y), tp: 2 (over core).
Axes of the slice: x: 2, y: 2, z: 4, core: 2. Of those that a mesh axis runs over, the one named last changes fastest.
Arguments:
- inputs: bfloat16 [4096, 2048], P(('rep', 'fs')), may hold values from -6 to 6
- cotangent: bfloat16 [4096, 2048], P(('rep', 'fs')), may hold values from -0.119628906 to 0.119628906
- up_weight: bfloat16 [2048, 4096], P('fs', 'tp'), may hold values from -0.125 to 0.125
- down_weight: bfloat16 [4096, 2048], P('tp', 'fs'), may hold values from -0.09375 to 0.09375
Outputs:
- grad_inputs: float32 [4096, 2048], P(('rep', 'fs'))
- grad_up: float32 [2048, 4096], P('fs', 'tp')
- grad_down: float32 [4096, 2048], P('tp', 'fs')
- norms_up: float32 [2048], P('fs')
- norms_down: float32 [4096], P('tp')
All inputs are finite; a program needn't handle non-finite values.
Results may differ from a plain program's by a relative error of at most 0.0029.
Values may be sent and summed in bfloat16 or wider, within the bound.
A program may use at most 128 MiB of HBM per device.

v0:
```python
import jax
import jax.numpy as jnp
from jax import lax
from jax.sharding import PartitionSpec as P


def contract(left, right, left_dim, right_dim):
    return lax.dot_general(
        left, right, (((left_dim,), (right_dim,)), ((), ())), preferred_element_type=jnp.float32
    )


def column_terms(left, right):
    return contract(left, right, 0, 0)


def shards(inputs, cotangent, up_weight, down_weight):
    up_whole = lax.all_gather(up_weight, "fs", axis=0, tiled=True)
    pre_act = jnp.dot(inputs, up_whole, preferred_element_type=jnp.float32)
    block = cotangent
    act_grad = contract(block, lax.all_gather(down_weight, "fs", axis=1, tiled=True), 1, 1)
    rectified = jnp.maximum(pre_act, 0.0)
    hidden = (rectified * rectified).astype(jnp.bfloat16)
    pre_grad = (2.0 * rectified * act_grad).astype(jnp.bfloat16)
    up_part = lax.psum_scatter(
        column_terms(inputs, pre_grad), "fs", scatter_dimension=0, tiled=True
    )
    down_part = lax.psum_scatter(
        column_terms(cotangent, hidden), "fs", scatter_dimension=0, tiled=True
    )
    grad_up, down_turned = lax.psum((up_part, down_part), "rep")
    block = pre_grad
    grad_inputs = lax.psum(contract(block, up_whole, 1, 1), "tp")
    norms_up = lax.psum(jnp.sum(grad_up * grad_up, axis=1), "tp")
    norms_down = lax.psum(jnp.sum(down_turned * down_turned, axis=0), "fs")
    grad_down = down_turned.T
    return (grad_inputs, grad_up, grad_down, norms_up, norms_down)


def solution(mesh):
    return jax.shard_map(
        shards,
        mesh=mesh,
        in_specs=(P(("rep", "fs"), None), P(("rep", "fs"), None), P("fs", "tp"), P("tp", "fs")),
        out_specs=(P(("rep", "fs"), None), P("fs", "tp"), P("tp", "fs"), P("fs"), P("tp")),
        check_vma=False,
    )
```

profile of v0, /device:TPU:0, one launch (start us, length us, event | category | flops | bytes accessed | tf_op | source)
XLA Modules:
  0.0 978.9 jit_solution(7159187467916872269)
XLA Ops:
  7.2 0.0 copy-start
  7.2 0.0 all-gather.3.cloned.1.call-start
  7.2 0.7 all-gather.3.cloned.1.call-update
  7.9 0.0 all-gather.5.cloned.1.call-start
  8.0 0.7 all-gather.5.cloned.1.call-update
  8.7 0.0 reduce-scatter.5.cloned.1.call-start
  8.7 128.6 %all-gather.3.cloned.1.call-done = bf16[2048,2048]{1,0:T(8,128)(2,1)} async-done(((bf16[256,2048]{1,0:T(8,128)(2,1)}), bf16[2048,2048]{1,0:T(8,128)(2,1)}) %all-gather.3.cloned.1.call-update) | async-done | bytes 8388624 | tf_op jit(solution)/shard_map/all_gather | solution.py:18
  137.3 6.1 convolution_maximum_fusion
  143.4 0.0 copy-done
  143.4 8.4 convolution_bitcast_fusion
  151.8 0.0 reduce-scatter.5.cloned.1.call-update
  151.8 0.0 reduce-scatter.3.cloned.1.call-start
  151.9 110.7 %all-gather.5.cloned.1.call-done = bf16[2048,2048]{1,0:T(8,128)(2,1)} async-done(((bf16[2048,256]{1,0:T(8,128)(2,1)}), bf16[2048,2048]{1,0:T(8,128)(2,1)}) %all-gather.5.cloned.1.call-update) | async-done | bytes 8388624 | tf_op jit(solution)/shard_map/all_gather | solution.py:21
  262.5 0.0 copy-start.3
  262.5 5.8 fusion
  268.4 0.0 copy-start.4
  268.4 1.0 copy-done.4
  269.4 0.0 copy-done.3
  269.4 8.1 convolution_bitcast_fusion.1
  277.5 0.0 reduce-scatter.3.cloned.1.call-update
  277.5 0.0 all-reduce.6.cloned.1.call-start
  277.5 267.2 %reduce-scatter.5.cloned.1.call-done = f32[256,2048]{0,1:T(8,128)} async-done(((f32[2048,2048]{0,1:T(8,128)}), f32[256,2048]{0,1:T(8,128)}) %reduce-scatter.5.cloned.1.call-update) | async-done | bytes 2097168 | tf_op jit(solution)/shard_map/reduce_scatter | solution.py:28
  544.7 282.9 %reduce-scatter.3.cloned.1.call-done = f32[256,2048]{0,1:T(8,128)} async-done(((f32[2048,2048]{0,1:T(8,128)}), f32[256,2048]{0,1:T(8,128)}) %reduce-scatter.3.cloned.1.call-update) | async-done | bytes 2097168 | tf_op jit(solution)/shard_map/reduce_scatter | solution.py:25
  827.6 0.0 copy-start.5
  827.6 0.0 all-reduce.6.cloned.1.call-update
  827.7 0.0 all-reduce.4.cloned.1.call-start
  827.7 1.2 copy-done.5
  828.9 7.1 fusion.1
  835.9 0.0 all-reduce.4.cloned.1.call-update
  836.0 101.1 %all-reduce.6.cloned.1.call-done = (f32[256,2048]{0,1:T(8,128)}, f32[256,2048]{0,1:T(8,128)}) async-done(((f32[256,2048]{0,1:T(8,128)}, f32[256,2048]{0,1:T(8,128)}), (f32[256,2048]{0,1:T(8,128)}, f32[256,2048]{0,1:T(8,128)})) %all-reduce.6.cloned.1.call-update) | async-done | bytes 4194320 | tf_op jit(solution)/shard_map/psum | solution.py:31
  937.0 2.9 copy.9
  939.9 0.0 copy-start.2
  939.9 2.0 multiply_reduce_fusion.1
  941.9 3.0 psum.38
  944.9 0.0 copy-done.2
  944.9 0.3 multiply_reduce_fusion
  945.3 22.2 %psum.39 = f32[2048]{0:T(1024)} all-reduce(f32[2048]{0:T(1024)S(1)} %multiply_reduce_fusion), channel_id=1, replica_groups=mesh['rep'=2,'fs'=8,'tp'=2] {'fs'}, use_global_device_ids=true, to_apply=%region_8.0 | all-reduce | flops 2048 | bytes 16384 | tf_op jit(solution)/shard_map/psum | solution.py:35
  967.5 0.0 all-reduce.4.cloned.1.call-done
  967.5 0.0 copy-start.1
  967.5 3.2 copy.13
  970.7 1.3 copy.14
  972.0 0.0 copy-done.1
Async XLA Ops:
  7.2 136.2 %copy-start = (bf16[256,2048]{1,0:T(8,128)(2,1)S(1)}, bf16[256,2048]{1,0:T(8,128)(2,1)}, u32[]{:S(2)}) copy-start(bf16[256,2048]{1,0:T(8,128)(2,1)} %param.5) | copy-start | bytes 3145732
  7.2 130.2 %all-gather.3.cloned.1.call-start = ((), (), s32[]{:S(2)}) async-start(), calls=%async_computation.2 | async-start | bytes 9437184 | tf_op jit(solution)/shard_map/all_gather | solution.py:18
  7.9 254.6 %all-gather.5.cloned.1.call-start = ((), (), s32[]{:S(2)}) async-start(), calls=%async_computation.3 | async-start | bytes 9437184 | tf_op jit(solution)/shard_map/all_gather | solution.py:21
  8.7 536.1 %reduce-scatter.5.cloned.1.call-start = ((), (), s32[]{:S(2)}) async-start(), calls=%async_computation.6 | async-start | bytes 18874368 | tf_op jit(solution)/shard_map/reduce_scatter | solution.py:28
  151.8 675.8 %reduce-scatter.3.cloned.1.call-start = ((), (), s32[]{:S(2)}) async-start(), calls=%async_computation.5 | async-start | bytes 18874368 | tf_op jit(solution)/shard_map/reduce_scatter | solution.py:25
  262.5 6.8 copy-start.3
  268.4 1.0 copy-start.4
  277.5 659.5 %all-reduce.6.cloned.1.call-start = ((), (), s32[]{:S(2)}) async-start(), calls=%async_computation.7 | async-start | bytes 8388608 | tf_op jit(solution)/shard_map/psum | solution.py:31
  827.6 1.2 copy-start.5
  827.7 139.8 %all-reduce.4.cloned.1.call-start = ((), (), s32[]{:S(2)}) async-start(), calls=%async_computation.4 | async-start | bytes 4194304 | tf_op jit(solution)/shard_map/psum | solution.py:33
  939.9 5.1 copy-start.2
  967.5 4.5 copy-start.1
Sparse Core Ops, SparseCore 0:
  10.1 127.1 all-gather.2
  139.4 123.1 all-gather.4
  266.3 278.3 reduce-scatter.4
  548.4 279.2 reduce-scatter.2
  830.0 106.9 all-reduce.5
  939.8 21.3 all-reduce.3
where the time goes:
time: 979 us
  waiting for transfers between devices  892 us (91%)
  matrix products  35.4 us (4%)
  blocking collectives  25.2 us (3%)
  between operations  14.2 us (1%)
    reduce_scatter x1, waiting for transfers between devices, shards(): lax.psum_scatter(column_terms(inputs, pre_grad), 'fs', scatter_dimension=...  283 us
    reduce_scatter x1, waiting for transfers between devices, shards(): lax.psum_scatter(column_terms(cotangent, hidden), 'fs', scatter_dimension...  267 us
    all_gather x1, waiting for transfers between devices, shards(): up_whole = lax.all_gather(up_weight, 'fs', axis=0, tiled=True)  129 us
    all_gather x1, waiting for transfers between devices, shards(): lax.all_gather(down_weight, 'fs', axis=1, tiled=True)  111 us
    psum x1, waiting for transfers between devices, shards(): grad_up, down_turned = lax.psum((up_part, down_part), 'rep')  101 us
    dot_general x4, matrix products, contract(): lax.dot_general(left, right, (((left_dim,), (right_dim,)), ((), ())), pre...  29.4 us
    psum x1, blocking collectives, shards(): norms_down = lax.psum(jnp.sum(down_turned * down_turned, axis=0), 'fs')  22.2 us
  transfers between devices with their start and end apart: 6, of which 5 were waited for; matrix products, arithmetic and copies ran while one was open for 4% of the time, Pallas kernels for 0%

commit v1 on v0

v1 whole, which is shorter than its diff:
```python
import jax
import jax.numpy as jnp
from jax import lax
from jax.sharding import PartitionSpec as P

NARROW = jnp.bfloat16


def contract(left, right, left_dim, right_dim):
    return lax.dot_general(
        left, right, (((left_dim,), (right_dim,)), ((), ())), preferred_element_type=jnp.float32
    )


def own_rows(block, axis):
    rows = block.shape[0] // lax.axis_size(axis)
    return lax.dynamic_slice_in_dim(block, lax.axis_index(axis) * rows, rows, 0)


def exchange(blocks, axis):
    return lax.all_to_all(blocks, axis, 0, 0)


def scatter_sum(blocks, axis):
    return jnp.sum(exchange(blocks.astype(NARROW), axis).astype(jnp.float32), axis=0)


def token_plan(inputs, cotangent, up_weight, down_weight):
    reps, groups, cores = (lax.axis_size(axis) for axis in ("rep", "fs", "tp"))
    rows, width = inputs.shape
    depth, units = up_weight.shape
    mine = units // groups
    part = depth // reps

    up = exchange(up_weight.reshape(depth, groups, mine).transpose(1, 0, 2), "fs")
    up = up.reshape(width, mine)
    down = exchange(down_weight.reshape(groups, mine, depth), "fs")
    down = down.transpose(1, 0, 2).reshape(mine, width)
    tokens = lax.all_gather(own_rows(inputs, "tp"), ("fs", "tp"), axis=0, tiled=True)
    cot = lax.all_gather(own_rows(cotangent, "tp"), ("fs", "tp"), axis=0, tiled=True)

    pre_act = contract(tokens, up, 1, 0)
    act_grad = contract(cot, down, 1, 1)
    rectified = jnp.maximum(pre_act, 0.0)
    hidden = (rectified * rectified).astype(jnp.bfloat16)
    pre_grad = (2.0 * rectified * act_grad).astype(jnp.bfloat16)

    share = contract(pre_grad, up, 1, 1)
    share = share.reshape(groups, cores, rows // cores, width).transpose(1, 0, 2, 3)
    share = scatter_sum(share, "tp")
    share = scatter_sum(share, "fs")
    grad_inputs = lax.all_gather(share, "tp", axis=0, tiled=True)

    def whole_gradient(term):
        term = term.reshape(groups, reps, part, mine).transpose(1, 0, 2, 3)
        term = scatter_sum(term, "rep")
        term = exchange(term.astype(NARROW), "fs")
        term = lax.all_gather(term, "rep", axis=0)
        return term.transpose(0, 2, 1, 3).reshape(depth, units).astype(jnp.float32)

    grad_up = whole_gradient(contract(tokens, pre_grad, 0, 0))
    down_turned = whole_gradient(contract(cot, hidden, 0, 0))
    norms_up = lax.psum(jnp.sum(grad_up * grad_up, axis=1), "tp")
    norms_down = lax.psum(jnp.sum(down_turned * down_turned, axis=0), "fs")
    return (grad_inputs, grad_up, down_turned.T, norms_up, norms_down)


def weight_plan(inputs, cotangent, up_weight, down_weight):
    up_whole = lax.all_gather(up_weight, "fs", axis=0, tiled=True)
    pre_act = jnp.dot(inputs, up_whole, preferred_element_type=jnp.float32)
    act_grad = contract(cotangent, lax.all_gather(down_weight, "fs", axis=1, tiled=True), 1, 1)
    rectified = jnp.maximum(pre_act, 0.0)
    hidden = (rectified * rectified).astype(jnp.bfloat16)
    pre_grad = (2.0 * rectified * act_grad).astype(jnp.bfloat16)
    up_part = lax.psum_scatter(
        contract(inputs, pre_grad, 0, 0), "fs", scatter_dimension=0, tiled=True
    )
    down_part = lax.psum_scatter(
        contract(cotangent, hidden, 0, 0), "fs", scatter_dimension=0, tiled=True
    )
    grad_up, down_turned = lax.psum((up_part, down_part), "rep")
    grad_inputs = lax.psum(contract(pre_grad, up_whole, 1, 1), "tp")
    norms_up = lax.psum(jnp.sum(grad_up * grad_up, axis=1), "tp")
    norms_down = lax.psum(jnp.sum(down_turned * down_turned, axis=0), "fs")
    grad_down = down_turned.T
    return (grad_inputs, grad_up, grad_down, norms_up, norms_down)


def shards(inputs, cotangent, up_weight, down_weight):
    tokens = inputs.size * lax.axis_size("fs") // lax.axis_size("tp")
    weights = up_weight.size * lax.axis_size("fs")
    plan = token_plan if tokens <= weights else weight_plan
    return plan(inputs, cotangent, up_weight, down_weight)


def solution(mesh):
    return jax.shard_map(
        shards,
        mesh=mesh,
        in_specs=(P(("rep", "fs"), None), P(("rep", "fs"), None), P("fs", "tp"), P("tp", "fs")),
        out_specs=(P(("rep", "fs"), None), P("fs", "tp"), P("tp", "fs"), P("fs"), P("tp")),
        check_vma=False,
    )
```

time: 979 us -> 460 us (0.47)
  waiting for transfers between devices: 892 us -> 298 us
  starting transfers between devices: 0.24 us -> 30.4 us
  local copies, waits for them, and re-layouts: 9.56 us -> 28.2 us
  blocking collectives: 25.2 us -> 41.8 us
  other arithmetic: 2.37 us -> 18.3 us
    reduce_scatter x2 -> x0, waiting for transfers between devices: 550 us -> none  [the longest x1 283 us: shards(): lax.psum_scatter(column_terms(inputs, pre_grad), 'fs', scatter_dimension=...]
    all_to_all x0 -> x7, waiting for transfers between devices: none -> 222 us  [exchange(): return lax.all_to_all(blocks, axis, 0, 0)]
    all_gather x2 -> x5, waiting for transfers between devices: 239 us -> 75.4 us  [the longest x1 69 us: token_plan(): lax.all_gather(own_rows(cotangent, 'tp'), ('fs', 'tp'), axis=0, tiled=True)]
    psum x2 -> x0, waiting for transfers between devices: 101 us -> none  [the longest x1 101 us: shards(): grad_up, down_turned = lax.psum((up_part, down_part), 'rep')]
    all_to_all x0 -> x7, starting transfers between devices: none -> 30 us  [exchange(): return lax.all_to_all(blocks, axis, 0, 0)]
    all_to_all x0 -> x1, blocking collectives: none -> 18.5 us  [exchange(): return lax.all_to_all(blocks, axis, 0, 0)]
    reduce_sum x2 -> x6, other arithmetic: 2.37 us -> 16.7 us  [the longest x4 14.9 us: scatter_sum(): jnp.sum(exchange(blocks.astype(NARROW), axis).astype(jnp.float32), axis=0)]
    convert_element_type x0 -> x4, local copies, waits for them, and re-layouts: none -> 11.6 us  [the longest x3 10.4 us: scatter_sum(): blocks.astype(NARROW)]
  transfers between devices with their start and end apart: 6 -> 12, of which waited for: 5 -> 9; matrix products, arithmetic and copies ran while one was open for 4% -> 9% of each run, Pallas kernels for 0% -> 0%
where the time goes in v1:
time: 460 us; the launch traced here: 459 us
  waiting for transfers between devices  298 us (65%)
  blocking collectives  41.8 us (9%)
  starting transfers between devices  30.4 us (7%)
  local copies, waits for them, and re-layouts  28.2 us (6%)
  matrix products  27.6 us (6%)
  other arithmetic  18.3 us (4%)
  between operations  14 us (3%)
    all_to_all x7, waiting for transfers between devices, exchange(): return lax.all_to_all(blocks, axis, 0, 0)  222 us
    all_gather x1, waiting for transfers between devices, token_plan(): lax.all_gather(own_rows(cotangent, 'tp'), ('fs', 'tp'), axis=0, tiled=True)  69 us
    all_to_all x7, starting transfers between devices, exchange(): return lax.all_to_all(blocks, axis, 0, 0)  30 us
    dot_general x5, matrix products, contract(): lax.dot_general(left, right, (((left_dim,), (right_dim,)), ((), ())), pre...  27.6 us
    psum x1, blocking collectives, token_plan(): norms_down = lax.psum(jnp.sum(down_turned * down_turned, axis=0), 'fs')  20.3 us
    all_to_all x1, blocking collectives, exchange(): return lax.all_to_all(blocks, axis, 0, 0)  18.5 us
    reduce_sum x4, other arithmetic, scatter_sum(): jnp.sum(exchange(blocks.astype(NARROW), axis).astype(jnp.float32), axis=0)  14.9 us
    unnamed x23, local copies, waits for them, and re-layouts  11 us
  transfers between devices with their start and end apart: 12, of which 9 were waited for; matrix products, arithmetic and copies ran while one was open for 9% of the time, Pallas kernels for 0%

profile of v1, /device:TPU:0, one launch (start us, length us, event | category | flops | bytes accessed | tf_op | source)
XLA Modules:
  0.0 458.6 jit_solution(16818338389971740752)
XLA Ops:
  7.2 1.2 copy-done
  8.4 0.8 constant_dynamic-slice_fusion.1
  9.3 2.0 constant_dynamic-slice_fusion
  11.3 7.3 %all-to-all-start.1 = ((bf16[8,256,256]{2,1,0:T(8,128)(2,1)}), bf16[8,256,256]{2,1,0:T(8,128)(2,1)S(1)}, u32[]{:S(2)}, u32[]{:S(2)}) async-start(bf16[8,256,256]{2,1,0:T(8,128)(2,1)} %bitcast.2), calls=%async_computation.1 | async-start | bytes 2097152 | tf_op jit(solution)/shard_map/all_to_all | solution.py:21
  18.6 1.0 copy.40
  19.7 41.6 %all-to-all-done.1 = bf16[8,256,256]{2,1,0:T(8,128)(2,1)S(1)} async-done(((bf16[8,256,256]{2,1,0:T(8,128)(2,1)}), bf16[8,256,256]{2,1,0:T(8,128)(2,1)S(1)}, u32[]{:S(2)}, u32[]{:S(2)}) %all-to-all-start.1) | async-done | bytes 1048608 | tf_op jit(solution)/shard_map/all_to_all | solution.py:21
  61.2 3.6 all-to-all-start
  64.9 0.5 copy.25
  65.4 53.2 %all-to-all-done = bf16[8,256,256]{2,1,0:T(8,128)(2,1)S(1)} async-done(((bf16[8,256,256]{2,1,0:T(8,128)(2,1)}), bf16[8,256,256]{2,1,0:T(8,128)(2,1)S(1)}, u32[]{:S(2)}, u32[]{:S(2)}) %all-to-all-start) | async-done | bytes 1048608 | tf_op jit(solution)/shard_map/all_to_all | solution.py:21
  118.6 6.3 %all-gather.8.cloned.1.call-done = bf16[2048,2048]{1,0:T(8,128)(2,1)} async-done(((bf16[128,2048]{1,0:T(8,128)(2,1)}), bf16[2048,2048]{1,0:T(8,128)(2,1)}) %all-gather.8.cloned.1.call-update) | async-done | bytes 8388624 | tf_op jit(solution)/shard_map/all_gather | solution.py:39
  125.0 7.1 %convolution_maximum_fusion = f32[2048,256]{1,0:T(8,128)} fusion(bf16[2048,2048]{1,0:T(8,128)(2,1)} %all-gather.8.cloned.1.call-done, bf16[2048,256]{1,0:T(8,128)(2,1)S(1)} %bitcast.61), kind=kOutput, calls=%fused_computation.3 | convolution fusion | flops 2148007936 | bytes 11534336 | tf_op jit(solution)/shard_map/dot_general | solution.py:10
  132.0 69.0 %all-gather.10.cloned.1.call-done = bf16[2048,2048]{1,0:T(8,128)(2,1)} async-done(((bf16[128,2048]{1,0:T(8,128)(2,1)}), bf16[2048,2048]{1,0:T(8,128)(2,1)}) %all-gather.10.cloned.1.call-update) | async-done | bytes 8388624 | tf_op jit(solution)/shard_map/all_gather | solution.py:40
  201.0 6.6 %convolution_convert_fusion = bf16[2048,256]{1,0:T(8,128)(2,1)S(1)} fusion(bf16[2048,2048]{1,0:T(8,128)(2,1)} %all-gather.10.cloned.1.call-done, f32[2048,256]{1,0:T(8,128)} %convolution_maximum_fusion), kind=kOutput, calls=%fused_computation.9 | convolution fusion | flops 2149056512 | bytes 11534336 | tf_op jit(solution)/shard_map/dot_general | solution.py:10
  207.7 1.0 copy.41
  208.7 0.9 copy-done.8
  209.6 2.4 fusion
  212.0 5.6 %convert_bitcast_fusion = bf16[2,8,128,2048]{3,2,0,1:T(8,128)(2,1)} fusion(bf16[8,2,128,256]{3,2,1,0:T(8,128)(2,1)S(1)} %bitcast.65, bf16[2048,256,1,1]{1,0,3,2:T(8,128)(2,1)S(1)} %bitcast.62), kind=kOutput, calls=%fused_computation.1 | convolution fusion | flops 2151677952 | bytes 10485760 | tf_op jit(solution)/shard_map/dot_general | solution.py:10
  217.6 8.3 %copy.26 = bf16[2,8,128,2048]{3,2,1,0:T(8,128)(2,1)} copy(bf16[2,8,128,2048]{3,2,0,1:T(8,128)(2,1)} %convert_bitcast_fusion) | data formatting | bytes 16777216 | tf_op jit(solution)/shard_map/convert_element_type | solution.py:25
  225.9 18.5 %all_to_all.40 = bf16[2,8,128,2048]{3,2,1,0:T(8,128)(2,1)} all-to-all(bf16[2,8,128,2048]{3,2,1,0:T(8,128)(2,1)} %copy.26), channel_id=1, replica_groups=mesh['rep'=2,'fs'=8,'tp'=2] {'tp'}, dimensions={0} | all-to-all | bytes 16777216 | tf_op jit(solution)/shard_map/all_to_all | solution.py:21
  244.4 3.8 all-to-all-start.6
  248.1 5.9 %convolution_convert_fusion.1 = bf16[2048,256]{1,0:T(8,128)(2,1)S(1)} fusion(bf16[2048,2048]{1,0:T(8,128)(2,1)} %all-gather.8.cloned.1.call-done, bf16[2048,256]{1,0:T(8,128)(2,1)S(1)} %fusion), kind=kOutput, calls=%fused_computation.10 | convolution fusion | flops 2148007936 | bytes 10485760 | tf_op jit(solution)/shard_map/dot_general | solution.py:10
  254.0 1.1 copy.42
  255.1 7.0 %all-to-all-done.6 = bf16[2,8,128,256]{3,2,1,0:T(8,128)(2,1)S(1)} async-done(((bf16[2,8,128,256]{3,2,1,0:T(8,128)(2,1)}), bf16[2,8,128,256]{3,2,1,0:T(8,128)(2,1)S(1)}, u32[]{:S(2)}, u32[]{:S(2)}) %all-to-all-start.6) | async-done | bytes 1048608 | tf_op jit(solution)/shard_map/all_to_all | solution.py:21
  262.1 3.6 all-to-all-start.4
  265.7 1.1 reduce_sum.70
  266.8 12.2 %all-to-all-done.4 = bf16[2,8,128,256]{3,2,1,0:T(8,128)(2,1)S(1)} async-done(((bf16[2,8,128,256]{3,2,1,0:T(8,128)(2,1)}), bf16[2,8,128,256]{3,2,1,0:T(8,128)(2,1)S(1)}, u32[]{:S(2)}, u32[]{:S(2)}) %all-to-all-start.4) | async-done | bytes 1048608 | tf_op jit(solution)/shard_map/all_to_all | solution.py:21
  279.0 3.5 all-to-all-start.7
  282.5 1.1 reduce_sum.69
  283.6 12.2 %all-to-all-done.7 = bf16[8,128,256]{2,1,0:T(8,128)(2,1)S(1)} async-done(((bf16[8,128,256]{2,1,0:T(8,128)(2,1)}), bf16[8,128,256]{2,1,0:T(8,128)(2,1)S(1)}, u32[]{:S(2)}, u32[]{:S(2)}) %all-to-all-start.7) | async-done | bytes 524320 | tf_op jit(solution)/shard_map/all_to_all | solution.py:21
  295.8 3.7 all-to-all-start.5
  299.5 8.7 %reduce_sum.67 = bf16[8,128,2048]{2,1,0:T(8,128)(2,1)} reduce(bf16[2,8,128,2048]{3,2,1,0:T(8,128)(2,1)} %all_to_all.40, bf16[]{:T(256)} %constant.18.clone.1), dimensions={0}, to_apply=%region_0.0 | reduce | flops 2097152 | bytes 12582914 | tf_op jit(solution)/shard_map/reduce_sum | solution.py:25
  308.2 5.1 %all-to-all-done.5 = bf16[8,128,256]{2,1,0:T(8,128)(2,1)S(1)} async-done(((bf16[8,128,256]{2,1,0:T(8,128)(2,1)}), bf16[8,128,256]{2,1,0:T(8,128)(2,1)S(1)}, u32[]{:S(2)}, u32[]{:S(2)}) %all-to-all-start.5) | async-done | bytes 524320 | tf_op jit(solution)/shard_map/all_to_all | solution.py:21
  313.3 0.8 copy-done.5
  314.1 4.6 all-to-all-start.3
  318.7 0.7 all-gather.16.cloned.1.call-update
  319.4 0.5 all-gather.14.cloned.1.call-update
  320.2 90.4 %all-to-all-done.3 = bf16[8,128,2048]{2,1,0:T(8,128)(2,1)} async-done(((bf16[8,128,2048]{2,1,0:T(8,128)(2,1)}), bf16[8,128,2048]{2,1,0:T(8,128)(2,1)}, u32[]{:S(2)}, u32[]{:S(2)}) %all-to-all-start.3) | async-done | bytes 4194336 | tf_op jit(solution)/shard_map/all_to_all | solution.py:21
  410.6 4.0 convert_reduce_fusion
  414.7 1.4 fusion.2
  416.1 1.4 convert_bitcast_fusion.2
  417.6 1.2 copy.28
  418.8 2.2 copy.34
  421.3 1.2 copy.30
  422.5 0.9 copy.35
  423.4 1.8 copy.31
  425.5 3.0 psum.14
  428.5 20.3 %psum.15 = f32[2048]{0:T(1024)} all-reduce(f32[2048]{0:T(1024)S(1)} %bitcast.71), channel_id=1, replica_groups=mesh['rep'=2,'fs'=8,'tp'=2] {'fs'}, use_global_device_ids=true, to_apply=%region_7.0 | all-reduce | flops 2048 | bytes 16384 | tf_op jit(solution)/shard_map/psum | solution.py:64
  448.8 3.2 copy.44
  (29 shorter events, 1.1 us)
Async XLA Ops:
  7.2 1.2 copy-start
  7.2 117.8 %all-gather.8.cloned.1.call-start = ((), (), s32[]{:S(2)}) async-start(), calls=%async_computation.8 | async-start | bytes 8912896 | tf_op jit(solution)/shard_map/all_gather | solution.py:39
  9.2 9.4 %copy-start.6 = (bf16[256,2048]{1,0:T(8,128)(2,1)S(1)}, bf16[256,2048]{1,0:T(8,128)(2,1)}, u32[]{:S(2)}) copy-start(bf16[256,2048]{1,0:T(8,128)(2,1)} %param.6) | copy-start | bytes 3145732
  9.3 191.7 %all-gather.10.cloned.1.call-start = ((), (), s32[]{:S(2)}) async-start(), calls=%async_computation.9 | async-start | bytes 8912896 | tf_op jit(solution)/shard_map/all_gather | solution.py:40
  11.3 49.9 %all-to-all-start.1 = ((bf16[8,256,256]{2,1,0:T(8,128)(2,1)}), bf16[8,256,256]{2,1,0:T(8,128)(2,1)S(1)}, u32[]{:S(2)}, u32[]{:S(2)}) async-start(bf16[8,256,256]{2,1,0:T(8,128)(2,1)} %bitcast.2), calls=%async_computation.1 | async-start | bytes 2097152 | tf_op jit(solution)/shard_map/all_to_all | solution.py:21
  61.2 57.4 %all-to-all-start = ((bf16[8,256,256]{2,1,0:T(8,128)(2,1)}), bf16[8,256,256]{2,1,0:T(8,128)(2,1)S(1)}, u32[]{:S(2)}, u32[]{:S(2)}) async-start(bf16[8,256,256]{2,1,0:T(8,128)(2,1)} %bitcast.53), calls=%async_computation | async-start | bytes 2097152 | tf_op jit(solution)/shard_map/all_to_all | solution.py:21
  201.0 7.7 %copy-start.7 = (bf16[2048,2048]{1,0:T(8,128)(2,1)S(1)}, bf16[2048,2048]{1,0:T(8,128)(2,1)}, u32[]{:S(2)}) copy-start(bf16[2048,2048]{1,0:T(8,128)(2,1)} %all-gather.10.cloned.1.call-done) | copy-start | bytes 25165828
  207.6 2.0 copy-start.8
  244.4 17.7 %all-to-all-start.6 = ((bf16[2,8,128,256]{3,2,1,0:T(8,128)(2,1)}), bf16[2,8,128,256]{3,2,1,0:T(8,128)(2,1)S(1)}, u32[]{:S(2)}, u32[]{:S(2)}) async-start(bf16[2,8,128,256]{3,2,1,0:T(8,128)(2,1)} %bitcast.54), calls=%async_computation.6 | async-start | bytes 2097152 | tf_op jit(solution)/shard_map/all_to_all | solution.py:21
  262.1 16.9 %all-to-all-start.4 = ((bf16[2,8,128,256]{3,2,1,0:T(8,128)(2,1)}), bf16[2,8,128,256]{3,2,1,0:T(8,128)(2,1)S(1)}, u32[]{:S(2)}, u32[]{:S(2)}) async-start(bf16[2,8,128,256]{3,2,1,0:T(8,128)(2,1)} %bitcast.55), calls=%async_computation.4 | async-start | bytes 2097152 | tf_op jit(solution)/shard_map/all_to_all | solution.py:21
  279.0 16.8 %all-to-all-start.7 = ((bf16[8,128,256]{2,1,0:T(8,128)(2,1)}), bf16[8,128,256]{2,1,0:T(8,128)(2,1)S(1)}, u32[]{:S(2)}, u32[]{:S(2)}) async-start(bf16[8,128,256]{2,1,0:T(8,128)(2,1)} %reduce_sum.70), calls=%async_computation.7 | async-start | bytes 1048576 | tf_op jit(solution)/shard_map/all_to_all | solution.py:21
  295.8 12.4 %copy-start.4 = (bf16[8,128,256]{2,1,0:T(8,128)(2,1)}, bf16[8,128,256]{2,1,0:T(8,128)(2,1)S(1)}, u32[]{:S(2)}) copy-start(bf16[8,128,256]{2,1,0:T(8,128)(2,1)S(1)} %all-to-all-done.7) | copy-start | bytes 1572868
  295.8 17.5 %all-to-all-start.5 = ((bf16[8,128,256]{2,1,0:T(8,128)(2,1)}), bf16[8,128,256]{2,1,0:T(8,128)(2,1)S(1)}, u32[]{:S(2)}, u32[]{:S(2)}) async-start(bf16[8,128,256]{2,1,0:T(8,128)(2,1)} %reduce_sum.69), calls=%async_computation.5 | async-start | bytes 1048576 | tf_op jit(solution)/shard_map/all_to_all | solution.py:21
  313.3 0.8 copy-start.5
  314.1 96.5 %all-to-all-start.3 = ((bf16[8,128,2048]{2,1,0:T(8,128)(2,1)}), bf16[8,128,2048]{2,1,0:T(8,128)(2,1)}, u32[]{:S(2)}, u32[]{:S(2)}) async-start(bf16[8,128,2048]{2,1,0:T(8,128)(2,1)} %reduce_sum.67), calls=%async_computation.3 | async-start | bytes 8388608 | tf_op jit(solution)/shard_map/all_to_all | solution.py:21
  318.6 96.0 %all-gather.16.cloned.1.call-start = ((), (), s32[]{:S(2)}) async-start(), calls=%async_computation.12 | async-start | bytes 1572864 | tf_op jit(solution)/shard_map/all_gather | solution.py:58
  319.4 96.8 %all-gather.14.cloned.1.call-start = ((), (), s32[]{:S(2)}) async-start(), calls=%async_computation.11 | async-start | bytes 1572864 | tf_op jit(solution)/shard_map/all_gather | solution.py:58
  320.0 128.8 %all-gather.12.cloned.1.call-start = ((), (), s32[]{:S(2)}) async-start(), calls=%async_computation.10 | async-start | bytes 3145728 | tf_op jit(solution)/shard_map/all_gather | solution.py:52
  418.8 2.2 copy-start.2
  423.4 1.8 copy-start.3
  448.8 3.2 copy-start.1
Sparse Core Ops, SparseCore 0:
  10.7 114.1 all-gather.7
  127.7 73.2 all-gather.9
  321.6 21.6 all-gather.15
  345.2 21.2 all-gather.13
  414.7 8.6 all-gather.11

commit v2 on v1

--- a/solution.py
+++ b/solution.py
@@ -4,6 +4,7 @@
 from jax.sharding import PartitionSpec as P
 
 NARROW = jnp.bfloat16
+CHUNKS = 2
 
 
 def contract(left, right, left_dim, right_dim):
@@ -12,17 +13,81 @@
     )
 
 
-def own_rows(block, axis):
-    rows = block.shape[0] // lax.axis_size(axis)
-    return lax.dynamic_slice_in_dim(block, lax.axis_index(axis) * rows, rows, 0)
+def own_block(blocks, axis, shift=0):
+    size = lax.axis_size(axis)
+    return lax.dynamic_index_in_dim(
+        blocks, lax.rem(lax.axis_index(axis) + shift, size), 0, keepdims=False
+    )
+
+
+def rotate(block, axis, shift):
+    size = lax.axis_size(axis)
+    return lax.ppermute(block, axis, [(at, (at + shift) % size) for at in range(size)])
+
+
+def scatter_sum(blocks, axis):
+    total = own_block(blocks, axis)
+    for shift in range(1, lax.axis_size(axis)):
+        sent = own_block(blocks, axis, shift).astype(NARROW)
+        total = total + rotate(sent, axis, shift).astype(jnp.float32)
+    return total
+
+
+def gather_blocks(block, axis):
+    size = lax.axis_size(axis)
+    me = lax.axis_index(axis)
+    held = [block] + [rotate(block, axis, shift) for shift in range(1, size)]
+    placed = []
+    for at in range(size):
+        pick = held[0]
+        for shift in range(1, size):
+            pick = jnp.where(lax.rem(me - at + size, size) == shift, held[shift], pick)
+        placed.append(pick)
+    return jnp.stack(placed)
+
+
+def fs_sum(blocks):
+    groups = lax.axis_size("fs")
+    pair = 2 if groups % 2 == 0 else 1
+    far = groups // pair
+    me = lax.axis_index("fs")
+    blocks = blocks.reshape((far, pair) + blocks.shape[1:])
+
+    def near_block(shift):
+        return lax.dynamic_index_in_dim(
+            blocks, lax.rem(lax.rem(me, pair) + shift, pair), 1, keepdims=False
+        )
+
+    held = near_block(0)
+    for shift in range(1, pair):
+        perm = [(at, at - at % pair + (at + shift) % pair) for at in range(groups)]
+        got = lax.ppermute(near_block(shift).astype(NARROW), "fs", perm)
+        held = held + got.astype(jnp.float32)
+
+    def far_block(shift):
+        return lax.dynamic_index_in_dim(held, lax.rem(me // pair + shift, far), 0, keepdims=False)
+
+    total = far_block(0)
+    for shift in range(1, far):
+        perm = [(at, (at + shift * pair) % groups) for at in range(groups)]
+        got = lax.ppermute(far_block(shift).astype(NARROW), "fs", perm)
+        total = total + got.astype(jnp.float32)
+    return total
 
 
 def exchange(blocks, axis):
     return lax.all_to_all(blocks, axis, 0, 0)
 
 
-def scatter_sum(blocks, axis):
-    return jnp.sum(exchange(blocks.astype(NARROW), axis).astype(jnp.float32), axis=0)
+def small_sum(value, axis):
+    size = lax.axis_size(axis)
+    if size & (size - 1):
+        return lax.psum(value, axis)
+    bit = 1
+    while bit < size:
+        value = value + lax.ppermute(value, axis, [(at, at ^ bit) for at in range(size)])
+        bit *= 2
+    return value
 
 
 def token_plan(inputs, cotangent, up_weight, down_weight):
@@ -31,13 +96,22 @@
     depth, units = up_weight.shape
     mine = units // groups
     part = depth // reps
+    half = width // cores
 
-    up = exchange(up_weight.reshape(depth, groups, mine).transpose(1, 0, 2), "fs")
-    up = up.reshape(width, mine)
-    down = exchange(down_weight.reshape(groups, mine, depth), "fs")
-    down = down.transpose(1, 0, 2).reshape(mine, width)
-    tokens = lax.all_gather(own_rows(inputs, "tp"), ("fs", "tp"), axis=0, tiled=True)
-    cot = lax.all_gather(own_rows(cotangent, "tp"), ("fs", "tp"), axis=0, tiled=True)
+    few = mine // reps
+    up = own_block(up_weight.reshape(reps, part, groups, mine).transpose(0, 2, 1, 3), "rep")
+    down = own_block(down_weight.reshape(groups, reps, few, depth).transpose(1, 0, 2, 3), "rep")
+    both = jnp.concatenate([up, down.reshape(groups, part, mine)], axis=1)
+    both = gather_blocks(exchange(both, "fs"), "rep")
+    up = both[:, :, :part].transpose(1, 0, 2, 3).reshape(width, mine)
+    down = both[:, :, part:].reshape(reps, groups, few, depth)
+    down = down.transpose(0, 2, 1, 3).reshape(mine, width)
+    tokens = lax.all_gather(
+        own_block(inputs.reshape(cores, rows // cores, width), "tp"), ("fs", "tp"), axis=0, tiled=True
+    )
+    cot = lax.all_gather(
+        own_block(cotangent.reshape(cores, rows // cores, width), "tp"), ("fs", "tp"), axis=0, tiled=True
+    )
 
     pre_act = contract(tokens, up, 1, 0)
     act_grad = contract(cot, down, 1, 1)
@@ -45,23 +119,32 @@
     hidden = (rectified * rectified).astype(jnp.bfloat16)
     pre_grad = (2.0 * rectified * act_grad).astype(jnp.bfloat16)
 
-    share = contract(pre_grad, up, 1, 1)
-    share = share.reshape(groups, cores, rows // cores, width).transpose(1, 0, 2, 3)
-    share = scatter_sum(share, "tp")
-    share = scatter_sum(share, "fs")
-    grad_inputs = lax.all_gather(share, "tp", axis=0, tiled=True)
+    up_rows = up.reshape(cores, half, mine)
+    share = contract(pre_grad, own_block(up_rows, "tp"), 1, 1)
+    for shift in range(1, cores):
+        sent = contract(pre_grad, own_block(up_rows, "tp", shift), 1, 1).astype(NARROW)
+        share = share + rotate(sent, "tp", shift).astype(jnp.float32)
+    chunks = CHUNKS if half % (128 * CHUNKS) == 0 else 1
+    share = share.reshape(groups, rows, half)
+    step = half // chunks
+    share = jnp.concatenate(
+        [fs_sum(share[:, :, at * step : (at + 1) * step]) for at in range(chunks)], axis=1
+    )
+    share = gather_blocks(share, "tp")
+    grad_inputs = share.transpose(1, 0, 2).reshape(rows, width)
 
-    def whole_gradient(term):
+    def spread(term):
         term = term.reshape(groups, reps, part, mine).transpose(1, 0, 2, 3)
-        term = scatter_sum(term, "rep")
-        term = exchange(term.astype(NARROW), "fs")
-        term = lax.all_gather(term, "rep", axis=0)
+        return exchange(scatter_sum(term, "rep").astype(NARROW), "fs")
+
+    def whole(term):
+        term = gather_blocks(term, "rep")
         return term.transpose(0, 2, 1, 3).reshape(depth, units).astype(jnp.float32)
 
-    grad_up = whole_gradient(contract(tokens, pre_grad, 0, 0))
-    down_turned = whole_gradient(contract(cot, hidden, 0, 0))
-    norms_up = lax.psum(jnp.sum(grad_up * grad_up, axis=1), "tp")
-    norms_down = lax.psum(jnp.sum(down_turned * down_turned, axis=0), "fs")
+    down_turned = whole(spread(contract(cot, hidden, 0, 0)))
+    grad_up = whole(spread(contract(tokens, pre_grad, 0, 0)))
+    norms_up = small_sum(jnp.sum(grad_up * grad_up, axis=1), "tp")
+    norms_down = small_sum(jnp.sum(down_turned * down_turned, axis=0), "fs")
     return (grad_inputs, grad_up, down_turned.T, norms_up, norms_down)
 
 

time: 460 us -> 351 us (0.76)
  waiting for transfers between devices: 298 us -> 168 us
  starting transfers between devices: 30.4 us -> 38.8 us
  blocking collectives: 41.8 us -> 49.7 us
  matrix products: 27.6 us -> 32.5 us
    all_to_all x7 -> x2, waiting for transfers between devices: 222 us -> 0.01 us  [exchange(): return lax.all_to_all(blocks, axis, 0, 0)]
    ppermute x0 -> x19, waiting for transfers between devices: none -> 80.8 us  [the longest x7 44.5 us: rotate(): lax.ppermute(block, axis, [(at, (at + shift) % size) for at in range(size)])]
    all_to_all x1, blocking collectives: 18.5 us -> 49.7 us  [exchange(): return lax.all_to_all(blocks, axis, 0, 0)]
    ppermute x0 -> x19, starting transfers between devices: none -> 29 us  [the longest x6 11.3 us: fs_sum(): got = lax.ppermute(far_block(shift).astype(NARROW), 'fs', perm)]
    psum x2 -> x0, blocking collectives: 23.3 us -> none  [the longest x1 20.3 us: token_plan(): norms_down = lax.psum(jnp.sum(down_turned * down_turned, axis=0), 'fs')]
    all_to_all x7 -> x2, starting transfers between devices: 30 us -> 9.77 us  [exchange(): return lax.all_to_all(blocks, axis, 0, 0)]
    reduce_sum x6 -> x2, other arithmetic: 16.7 us -> 0.51 us  [the longest x1 0.29 us: token_plan(): norms_up = small_sum(jnp.sum(grad_up * grad_up, axis=1), 'tp')]
    all_gather x5 -> x2, waiting for transfers between devices: 75.4 us -> 87.1 us  [the longest x1 68.6 us: token_plan(): lax.all_gather(own_block(cotangent.reshape(cores, rows // cores, width),...]
  transfers between devices with their start and end apart: 12 -> 23, of which waited for: 9 -> 10; matrix products, arithmetic and copies ran while one was open for 9% -> 16% of each run, Pallas kernels for 0% -> 0%
where the time goes in v2:
time: 351 us; the launch traced here: 350 us
  waiting for transfers between devices  168 us (48%)
  blocking collectives  49.7 us (14%)
  starting transfers between devices  38.8 us (11%)
  matrix products  32.5 us (9%)
  local copies, waits for them, and re-layouts  26.8 us (8%)
  other arithmetic  19.6 us (6%)
  between operations  14.5 us (4%)
    all_gather x1, waiting for transfers between devices, token_plan(): lax.all_gather(own_block(cotangent.reshape(cores, rows // cores, width),...  68.6 us
    all_to_all x1, blocking collectives, exchange(): return lax.all_to_all(blocks, axis, 0, 0)  49.7 us
    ppermute x7, waiting for transfers between devices, rotate(): lax.ppermute(block, axis, [(at, (at + shift) % size) for at in range(size)])  44.5 us
    dot_general x6, matrix products, contract(): lax.dot_general(left, right, (((left_dim,), (right_dim,)), ((), ())), pre...  32.5 us
    all_gather x1, waiting for transfers between devices, token_plan(): lax.all_gather(own_block(inputs.reshape(cores, rows // cores, width), 'tp...  18.6 us
    ppermute x6, waiting for transfers between devices, fs_sum(): got = lax.ppermute(far_block(shift).astype(NARROW), 'fs', perm)  16.6 us
    ppermute x2, waiting for transfers between devices, fs_sum(): got = lax.ppermute(near_block(shift).astype(NARROW), 'fs', perm)  15.6 us
    unnamed x38, local copies, waits for them, and re-layouts  14 us
  transfers between devices with their start and end apart: 23, of which 10 were waited for; matrix products, arithmetic and copies ran while one was open for 16% of the time, Pallas kernels for 0%

profile of v2, /device:TPU:0, one launch (start us, length us, event | category | flops | bytes accessed | tf_op | source)
XLA Modules:
  0.0 349.8 jit_solution(14163850069657369304)
XLA Ops:
  9.3 2.0 constant_dynamic-slice_fusion
  12.4 49.7 %all_to_all.15 = bf16[8,256,256]{2,1,0:T(8,128)(2,1)S(1)} all-to-all(bf16[8,256,256]{2,1,0:T(8,128)(2,1)S(1)} %copy.33), channel_id=1, replica_groups=mesh['rep'=2,'fs'=8,'tp'=2] {'fs'}, dimensions={0} | all-to-all | bytes 2097152 | tf_op jit(solution)/shard_map/all_to_all | solution.py:79
  62.1 1.5 collective-permute-start
  63.6 22.0 %collective-permute-done = bf16[8,256,256]{2,1,0:T(8,128)(2,1)S(1)} collective-permute-done((bf16[8,256,256]{2,1,0:T(8,128)(2,1)S(1)}, bf16[8,256,256]{2,1,0:T(8,128)(2,1)S(1)}, u32[]{:S(2)}, u32[]{:S(2)}) %collective-permute-start) | collective-permute-done | bytes 1048608 | tf_op jit(solution)/shard_map/ppermute | solution.py:25
  86.8 18.6 %all-gather.5.cloned.1.call-done = bf16[1,2048,2048]{2,1,0:T(8,128)(2,1)} async-done(((bf16[1,128,2048]{2,1,0:T(8,128)(2,1)}), bf16[1,2048,2048]{2,1,0:T(8,128)(2,1)}) %all-gather.5.cloned.1.call-update) | async-done | bytes 8388624 | tf_op jit(solution)/shard_map/all_gather | solution.py:109
  105.4 7.1 %fusion.8 = f32[2048,256]{1,0:T(8,128)} fusion(bf16[2048,256]{1,0:T(8,128)(2,1)S(1)} %bitcast.161, bf16[1,2048,2048]{2,1,0:T(8,128)(2,1)} %all-gather.5.cloned.1.call-done), kind=kOutput, calls=%fused_computation.10 | convolution fusion | flops 2148007936 | bytes 11534336 | tf_op jit(solution)/shard_map/dot_general | solution.py:11
  112.5 68.6 %all-gather.7.cloned.1.call-done = bf16[1,2048,2048]{2,1,0:T(8,128)(2,1)} async-done(((bf16[1,128,2048]{2,1,0:T(8,128)(2,1)}), bf16[1,2048,2048]{2,1,0:T(8,128)(2,1)}) %all-gather.7.cloned.1.call-update) | async-done | bytes 8388624 | tf_op jit(solution)/shard_map/all_gather | solution.py:112
  181.0 6.4 %fusion.14 = bf16[2048,256]{1,0:T(8,128)(2,1)S(1)} fusion(bf16[256,2048]{1,0:T(8,128)(2,1)S(1)} %bitcast.174, bf16[1,2048,2048]{2,1,0:T(8,128)(2,1)} %all-gather.7.cloned.1.call-done, f32[2048,256]{1,0:T(8,128)} %fusion.8), kind=kOutput, calls=%fused_computation.16 | convolution fusion | flops 2149056512 | bytes 12582912 | tf_op jit(solution)/shard_map/dot_general | solution.py:11
  187.4 3.3 convolution_convert_fusion
  191.0 6.0 %fusion.4 = f32[2048,256]{1,0:T(8,128)S(1)} fusion(bf16[2048,256]{1,0:T(8,128)(2,1)S(1)} %fusion.14, bf16[1,2048,2048]{2,1,0:T(8,128)(2,1)} %all-gather.5.cloned.1.call-done), kind=kOutput, calls=%fused_computation.4 | convolution fusion | flops 2147483648 | bytes 11534336 | tf_op jit(solution)/shard_map/dot_general | solution.py:11
  197.0 1.3 copy-done.11
  198.3 1.5 collective-permute-start.11
  199.9 12.6 %collective-permute-done.11 = bf16[8,128,256]{2,1,0:T(8,128)(2,1)S(1)} collective-permute-done((bf16[8,128,256]{2,1,0:T(8,128)(2,1)S(1)}, bf16[8,128,256]{2,1,0:T(8,128)(2,1)S(1)}, u32[]{:S(2)}, u32[]{:S(2)}) %collective-permute-start.11) | collective-permute-done | bytes 524320 | tf_op jit(solution)/shard_map/ppermute | solution.py:25
  212.5 2.1 fusion.24
  214.6 4.3 %all-to-all-start.1 = ((bf16[8,128,256]{2,1,0:T(8,128)(2,1)}), bf16[8,128,256]{2,1,0:T(8,128)(2,1)}, u32[]{:S(2)}, u32[]{:S(2)}) async-start(bf16[8,128,256]{2,1,0:T(8,128)(2,1)} %fusion.24), calls=%async_computation.1 | async-start | bytes 1048576 | tf_op jit(solution)/shard_map/all_to_all | solution.py:79
  219.0 3.5 convert_add_fusion
  222.5 1.4 fusion.46
  224.1 1.8 collective-permute-start.2
  227.1 6.3 %fusion = f32[2048,256]{1,0:T(8,128)S(1)} fusion(bf16[1,2048,2048]{2,1,0:T(8,128)(2,1)} %all-gather.7.cloned.1.call-done, f32[2048,256]{1,0:T(8,128)S(1)} %copy-done.15), kind=kOutput, calls=%fused_computation | convolution fusion | flops 2148532224 | bytes 12582912 | tf_op jit(solution)/shard_map/dot_general | solution.py:11
  233.5 1.5 collective-permute-start.13
  235.2 1.8 collective-permute-start.6
  236.9 9.9 %collective-permute-done.13 = bf16[8,128,256]{2,1,0:T(8,128)(2,1)S(1)} collective-permute-done((bf16[8,128,256]{2,1,0:T(8,128)(2,1)S(1)}, bf16[8,128,256]{2,1,0:T(8,128)(2,1)S(1)}, u32[]{:S(2)}, u32[]{:S(2)}) %collective-permute-start.13) | collective-permute-done | bytes 524320 | tf_op jit(solution)/shard_map/ppermute | solution.py:25
  247.7 5.4 %all-to-all-start.2 = ((bf16[8,128,256]{2,1,0:T(8,128)(2,1)}), bf16[8,128,256]{2,1,0:T(8,128)(2,1)}, u32[]{:S(2)}, u32[]{:S(2)}) async-start(bf16[8,128,256]{2,1,0:T(8,128)(2,1)} %fusion.23), calls=%async_computation.2 | async-start | bytes 1048576 | tf_op jit(solution)/shard_map/all_to_all | solution.py:79
  253.2 2.5 bitcast_add_fusion.1
  256.5 2.0 collective-permute-start.3
  258.5 2.4 collective-permute-start.4
  260.9 1.5 collective-permute-start.5
  262.4 15.6 %collective-permute-done.6 = bf16[4,256,512]{2,1,0:T(8,128)(2,1)} collective-permute-done((bf16[4,256,512]{2,1,0:T(8,128)(2,1)S(1)}, bf16[4,256,512]{2,1,0:T(8,128)(2,1)}, u32[]{:S(2)}, u32[]{:S(2)}) %collective-permute-start.6) | collective-permute-done | bytes 1048608 | tf_op jit(solution)/shard_map/ppermute | solution.py:64
  278.0 1.6 bitcast_add_fusion
  281.7 1.6 collective-permute-start.7
  283.3 1.5 collective-permute-start.8
  285.5 2.4 collective-permute-start.9
  287.9 6.6 %collective-permute-done.4 = bf16[256,512]{1,0:T(8,128)(2,1)} collective-permute-done((bf16[256,512]{1,0:T(8,128)(2,1)}, bf16[256,512]{1,0:T(8,128)(2,1)}, u32[]{:S(2)}, u32[]{:S(2)}) %collective-permute-start.4) | collective-permute-done | bytes 262176 | tf_op jit(solution)/shard_map/ppermute | solution.py:73
  294.5 1.5 collective-permute-start.12
  297.8 10.0 %collective-permute-done.8 = bf16[256,512]{1,0:T(8,128)(2,1)} collective-permute-done((bf16[256,512]{1,0:T(8,128)(2,1)S(1)}, bf16[256,512]{1,0:T(8,128)(2,1)}, u32[]{:S(2)}, u32[]{:S(2)}) %collective-permute-start.8) | collective-permute-done | bytes 262176 | tf_op jit(solution)/shard_map/ppermute | solution.py:73
  307.8 1.4 fusion.28
  310.4 1.7 select_bitcast_fusion.4
  314.1 1.9 collective-permute-done.16
  316.0 4.0 %collective-permute-start.17 = (f32[2048]{0:T(1024)S(1)}, f32[2048]{0:T(1024)S(1)}, u32[]{:S(2)}, u32[]{:S(2)}) collective-permute-start(f32[2048]{0:T(1024)S(1)} %add.165), channel_id=1, source_target_pairs={{0,4},{2,6},{4,0},{6,2},{8,12},{10,14},{12,8},{14,10},{1,5},{3,7},... | collective-permute-start | bytes 24584 | tf_op jit(solution)/shard_map/ppermute | solution.py:88
  320.0 1.5 convert_bitcast_fusion.1
  321.5 2.3 copy.41
  323.8 3.2 copy.52
  328.2 2.2 copy.48
  330.4 1.9 collective-permute-start.18
  333.0 2.0 collective-permute-done.18
  335.6 1.4 select_bitcast_fusion
  338.8 1.9 pad_maximum_fusion
  340.7 2.2 copy.47
  (84 shorter events, 20.0 us)
Async XLA Ops:
  7.2 1.2 copy-start
  7.2 4.1 %copy-start.12 = (bf16[256,2048]{1,0:T(8,128)(2,1)S(1)}, bf16[256,2048]{1,0:T(8,128)(2,1)}, u32[]{:S(2)}) copy-start(bf16[256,2048]{1,0:T(8,128)(2,1)} %param.6) | copy-start | bytes 3145732
  7.2 98.2 %all-gather.5.cloned.1.call-start = ((), (), s32[]{:S(2)}) async-start(), calls=%async_computation.3 | async-start | bytes 8912896 | tf_op jit(solution)/shard_map/all_gather | solution.py:109
  9.2 2.4 copy-start.13
  9.3 171.8 %all-gather.7.cloned.1.call-start = ((), (), s32[]{:S(2)}) async-start(), calls=%async_computation.4 | async-start | bytes 8912896 | tf_op jit(solution)/shard_map/all_gather | solution.py:112
  62.1 23.5 %collective-permute-start = (bf16[8,256,256]{2,1,0:T(8,128)(2,1)S(1)}, bf16[8,256,256]{2,1,0:T(8,128)(2,1)S(1)}, u32[]{:S(2)}, u32[]{:S(2)}) collective-permute-start(bf16[8,256,256]{2,1,0:T(8,128)(2,1)S(1)} %all_to_all.15), channel_id=1, source_target_pairs={{0,16},{16,0},{1,17},{17,1},{2,18},{18,2},{3,19},{19,3},{4,20},{20... | collective-permute-start | bytes 3145736 | tf_op jit(solution)/shard_map/ppermute | solution.py:25
  190.7 28.3 %collective-permute-start.1 = (bf16[2048,1024]{1,0:T(8,128)(2,1)}, bf16[2048,1024]{1,0:T(8,128)(2,1)}, u32[]{:S(2)}, u32[]{:S(2)}) collective-permute-start(bf16[2048,1024]{1,0:T(8,128)(2,1)} %convolution_convert_fusion), channel_id=1, source_target_pairs={{0,1},{1,0},{2,3},{3,2},{4,5},{5,4},{6,7},{7,6},{8,9},{9,8},{10,11... | collective-permute-start | bytes 12582920 | tf_op jit(solution)/shard_map/ppermute | solution.py:25
  197.0 1.3 copy-start.11
  198.3 14.2 %collective-permute-start.11 = (bf16[8,128,256]{2,1,0:T(8,128)(2,1)S(1)}, bf16[8,128,256]{2,1,0:T(8,128)(2,1)S(1)}, u32[]{:S(2)}, u32[]{:S(2)}) collective-permute-start(bf16[8,128,256]{2,1,0:T(8,128)(2,1)S(1)} %fusion.25), channel_id=1, source_target_pairs={{0,16},{16,0},{1,17},{17,1},{2,18},{18,2},{3,19},{19,3},{4,20},{20... | collective-permute-start | bytes 1572872 | tf_op jit(solution)/shard_map/ppermute | solution.py:25
  214.6 33.1 %all-to-all-start.1 = ((bf16[8,128,256]{2,1,0:T(8,128)(2,1)}), bf16[8,128,256]{2,1,0:T(8,128)(2,1)}, u32[]{:S(2)}, u32[]{:S(2)}) async-start(bf16[8,128,256]{2,1,0:T(8,128)(2,1)} %fusion.24), calls=%async_computation.1 | async-start | bytes 1048576 | tf_op jit(solution)/shard_map/all_to_all | solution.py:79
  223.9 9.5 %copy-start.4 = (f32[8,256,512]{2,1,0:T(8,128)}, f32[8,256,512]{2,1,0:T(8,128)S(1)}, u32[]{:S(2)}) copy-start(f32[8,256,512]{2,1,0:T(8,128)S(1)} %get-tuple-element.5) | copy-start | bytes 12582916
  223.9 11.1 %copy-start.2 = (f32[8,256,512]{2,1,0:T(8,128)}, f32[8,256,512]{2,1,0:T(8,128)S(1)}, u32[]{:S(2)}) copy-start(f32[8,256,512]{2,1,0:T(8,128)S(1)} %get-tuple-element.6) | copy-start | bytes 12582916
  223.9 3.2 copy-start.15
  224.1 29.1 %collective-permute-start.2 = (bf16[4,256,512]{2,1,0:T(8,128)(2,1)S(1)}, bf16[4,256,512]{2,1,0:T(8,128)(2,1)}, u32[]{:S(2)}, u32[]{:S(2)}) collective-permute-start(bf16[4,256,512]{2,1,0:T(8,128)(2,1)S(1)} %fusion.19), channel_id=1, source_target_pairs={{0,2},{2,0},{4,6},{6,4},{8,10},{10,8},{12,14},{14,12},{1,3},{3,1},... | collective-permute-start | bytes 3145736 | tf_op jit(solution)/shard_map/ppermute | solution.py:64
  233.5 13.3 %collective-permute-start.13 = (bf16[8,128,256]{2,1,0:T(8,128)(2,1)S(1)}, bf16[8,128,256]{2,1,0:T(8,128)(2,1)S(1)}, u32[]{:S(2)}, u32[]{:S(2)}) collective-permute-start(bf16[8,128,256]{2,1,0:T(8,128)(2,1)S(1)} %fusion.26), channel_id=1, source_target_pairs={{0,16},{16,0},{1,17},{17,1},{2,18},{18,2},{3,19},{19,3},{4,20},{20... | collective-permute-start | bytes 1572872 | tf_op jit(solution)/shard_map/ppermute | solution.py:25
  235.2 42.8 %collective-permute-start.6 = (bf16[4,256,512]{2,1,0:T(8,128)(2,1)S(1)}, bf16[4,256,512]{2,1,0:T(8,128)(2,1)}, u32[]{:S(2)}, u32[]{:S(2)}) collective-permute-start(bf16[4,256,512]{2,1,0:T(8,128)(2,1)S(1)} %fusion.20), channel_id=1, source_target_pairs={{0,2},{2,0},{4,6},{6,4},{8,10},{10,8},{12,14},{14,12},{1,3},{3,1},... | collective-permute-start | bytes 3145736 | tf_op jit(solution)/shard_map/ppermute | solution.py:64
  247.7 48.2 %all-to-all-start.2 = ((bf16[8,128,256]{2,1,0:T(8,128)(2,1)}), bf16[8,128,256]{2,1,0:T(8,128)(2,1)}, u32[]{:S(2)}, u32[]{:S(2)}) async-start(bf16[8,128,256]{2,1,0:T(8,128)(2,1)} %fusion.23), calls=%async_computation.2 | async-start | bytes 1048576 | tf_op jit(solution)/shard_map/all_to_all | solution.py:79
  253.2 24.8 %copy-start.3 = (f32[8,256,512]{2,1,0:T(8,128)S(1)}, f32[8,256,512]{2,1,0:T(8,128)}, u32[]{:S(2)}) copy-start(f32[8,256,512]{2,1,0:T(8,128)} %copy-done.2) | copy-start | bytes 12582916
  256.5 28.3 %collective-permute-start.3 = (bf16[256,512]{1,0:T(8,128)(2,1)S(1)}, bf16[256,512]{1,0:T(8,128)(2,1)S(1)}, u32[]{:S(2)}, u32[]{:S(2)}) collective-permute-start(bf16[256,512]{1,0:T(8,128)(2,1)S(1)} %get-tuple-element.9), channel_id=1, source_target_pairs={{0,4},{2,6},{4,8},{6,10},{8,12},{10,14},{12,0},{14,2},{1,5},{3,7},... | collective-permute-start | bytes 786440 | tf_op jit(solution)/shard_map/ppermute | solution.py:73
  258.5 36.0 %collective-permute-start.4 = (bf16[256,512]{1,0:T(8,128)(2,1)}, bf16[256,512]{1,0:T(8,128)(2,1)}, u32[]{:S(2)}, u32[]{:S(2)}) collective-permute-start(bf16[256,512]{1,0:T(8,128)(2,1)} %get-tuple-element.11), channel_id=1, source_target_pairs={{0,8},{2,10},{4,12},{6,14},{8,0},{10,2},{12,4},{14,6},{1,9},{3,11}... | collective-permute-start | bytes 786440 | tf_op jit(solution)/shard_map/ppermute | solution.py:73
  260.9 35.1 %collective-permute-start.5 = (bf16[256,512]{1,0:T(8,128)(2,1)S(1)}, bf16[256,512]{1,0:T(8,128)(2,1)}, u32[]{:S(2)}, u32[]{:S(2)}) collective-permute-start(bf16[256,512]{1,0:T(8,128)(2,1)S(1)} %get-tuple-element.10), channel_id=1, source_target_pairs={{0,12},{2,14},{4,0},{6,2},{8,4},{10,6},{12,8},{14,10},{1,13},{3,15... | collective-permute-start | bytes 786440 | tf_op jit(solution)/shard_map/ppermute | solution.py:73
  279.6 1.3 copy-start.6
  281.7 16.1 %collective-permute-start.7 = (bf16[256,512]{1,0:T(8,128)(2,1)}, bf16[256,512]{1,0:T(8,128)(2,1)}, u32[]{:S(2)}, u32[]{:S(2)}) collective-permute-start(bf16[256,512]{1,0:T(8,128)(2,1)} %get-tuple-element.12), channel_id=1, source_target_pairs={{0,4},{2,6},{4,8},{6,10},{8,12},{10,14},{12,0},{14,2},{1,5},{3,7},... | collective-permute-start | bytes 786440 | tf_op jit(solution)/shard_map/ppermute | solution.py:73
  283.3 24.5 %collective-permute-start.8 = (bf16[256,512]{1,0:T(8,128)(2,1)S(1)}, bf16[256,512]{1,0:T(8,128)(2,1)}, u32[]{:S(2)}, u32[]{:S(2)}) collective-permute-start(bf16[256,512]{1,0:T(8,128)(2,1)S(1)} %get-tuple-element.14), channel_id=1, source_target_pairs={{0,8},{2,10},{4,12},{6,14},{8,0},{10,2},{12,4},{14,6},{1,9},{3,11}... | collective-permute-start | bytes 786440 | tf_op jit(solution)/shard_map/ppermute | solution.py:73
  284.8 0.7 copy-start.14
  285.5 22.3 %collective-permute-start.9 = (bf16[256,512]{1,0:T(8,128)(2,1)S(1)}, bf16[256,512]{1,0:T(8,128)(2,1)}, u32[]{:S(2)}, u32[]{:S(2)}) collective-permute-start(bf16[256,512]{1,0:T(8,128)(2,1)S(1)} %get-tuple-element.13), channel_id=1, source_target_pairs={{0,12},{2,14},{4,0},{6,2},{8,4},{10,6},{12,8},{14,10},{1,13},{3,15... | collective-permute-start | bytes 786440 | tf_op jit(solution)/shard_map/ppermute | solution.py:73
  294.5 15.8 %collective-permute-start.12 = (bf16[8,128,256]{2,1,0:T(8,128)(2,1)}, bf16[8,128,256]{2,1,0:T(8,128)(2,1)}, u32[]{:S(2)}, u32[]{:S(2)}) collective-permute-start(bf16[8,128,256]{2,1,0:T(8,128)(2,1)} %all-to-all-done.1), channel_id=1, source_target_pairs={{0,16},{16,0},{1,17},{17,1},{2,18},{18,2},{3,19},{19,3},{4,20},{20... | collective-permute-start | bytes 1572872 | tf_op jit(solution)/shard_map/ppermute | solution.py:25
  296.0 14.4 %collective-permute-start.14 = (bf16[8,128,256]{2,1,0:T(8,128)(2,1)}, bf16[8,128,256]{2,1,0:T(8,128)(2,1)}, u32[]{:S(2)}, u32[]{:S(2)}) collective-permute-start(bf16[8,128,256]{2,1,0:T(8,128)(2,1)} %all-to-all-done.2), channel_id=1, source_target_pairs={{0,16},{16,0},{1,17},{17,1},{2,18},{18,2},{3,19},{19,3},{4,20},{20... | collective-permute-start | bytes 1572872 | tf_op jit(solution)/shard_map/ppermute | solution.py:25
  297.8 12.6 %copy-start.7 = (f32[256,512]{1,0:T(8,128)}, f32[256,512]{1,0:T(8,128)S(1)}, u32[]{:S(2)}) copy-start(f32[256,512]{1,0:T(8,128)S(1)} %fusion.30) | copy-start | bytes 1572868
  309.2 1.1 copy-start.9
  310.4 25.2 %collective-permute-start.10 = (f32[256,1024]{1,0:T(8,128)}, f32[256,1024]{1,0:T(8,128)}, u32[]{:S(2)}, u32[]{:S(2)}) collective-permute-start(f32[256,1024]{1,0:T(8,128)} %pad_maximum_fusion.3), channel_id=1, source_target_pairs={{0,1},{1,0},{2,3},{3,2},{4,5},{5,4},{6,7},{7,6},{8,9},{9,8},{10,11... | collective-permute-start | bytes 3145736 | tf_op jit(solution)/shard_map/ppermute | solution.py:25
  312.3 3.7 %collective-permute-start.16 = (f32[2048]{0:T(1024)S(1)}, f32[2048]{0:T(1024)S(1)}, u32[]{:S(2)}, u32[]{:S(2)}) collective-permute-start(f32[2048]{0:T(1024)S(1)} %bitcast.178), channel_id=1, source_target_pairs={{0,2},{2,0},{4,6},{6,4},{8,10},{10,8},{12,14},{14,12},{1,3},{3,1},... | collective-permute-start | bytes 24584 | tf_op jit(solution)/shard_map/ppermute | solution.py:88
  313.8 18.6 %collective-permute-start.15 = (f32[256]{0:T(256)S(1)}, f32[256]{0:T(256)S(1)}, u32[]{:S(2)}, u32[]{:S(2)}) collective-permute-start(f32[256]{0:T(256)S(1)} %bitcast.180), channel_id=1, source_target_pairs={{0,1},{1,0},{2,3},{3,2},{4,5},{5,4},{6,7},{7,6},{8,9},{9,8},{10,11... | collective-permute-start | bytes 3080 | tf_op jit(solution)/shard_map/ppermute | solution.py:88
  316.0 14.4 %collective-permute-start.17 = (f32[2048]{0:T(1024)S(1)}, f32[2048]{0:T(1024)S(1)}, u32[]{:S(2)}, u32[]{:S(2)}) collective-permute-start(f32[2048]{0:T(1024)S(1)} %add.165), channel_id=1, source_target_pairs={{0,4},{2,6},{4,0},{6,2},{8,12},{10,14},{12,8},{14,10},{1,5},{3,7},... | collective-permute-start | bytes 24584 | tf_op jit(solution)/shard_map/ppermute | solution.py:88
  323.8 3.2 copy-start.5
  328.2 7.4 %copy-start.8 = (f32[256,512]{1,0:T(8,128)S(1)}, f32[256,512]{1,0:T(8,128)}, u32[]{:S(2)}) copy-start(f32[256,512]{1,0:T(8,128)} %copy-done.7) | copy-start | bytes 1572868
  328.2 7.4 %copy-start.10 = (f32[256,512]{1,0:T(8,128)S(1)}, f32[256,512]{1,0:T(8,128)}, u32[]{:S(2)}) copy-start(f32[256,512]{1,0:T(8,128)} %copy-done.9) | copy-start | bytes 1572868
  330.4 4.6 %collective-permute-start.18 = (f32[2048]{0:T(1024)S(1)}, f32[2048]{0:T(1024)S(1)}, u32[]{:S(2)}, u32[]{:S(2)}) collective-permute-start(f32[2048]{0:T(1024)S(1)} %add.166), channel_id=1, source_target_pairs={{0,8},{2,10},{4,12},{6,14},{8,0},{10,2},{12,4},{14,6},{1,9},{3,11}... | collective-permute-start | bytes 24584 | tf_op jit(solution)/shard_map/ppermute | solution.py:88
  340.7 2.2 copy-start.1
Sparse Core Ops, SparseCore 0:
  10.7 94.6 all-gather.4
  108.1 72.8 all-gather.6

commit v3 on v2

--- a/solution.py
+++ b/solution.py
@@ -46,7 +46,7 @@
     return jnp.stack(placed)
 
 
-def fs_sum(blocks):
+def fs_sum(blocks, ahead=None):
     groups = lax.axis_size("fs")
     pair = 2 if groups % 2 == 0 else 1
     far = groups // pair
@@ -64,6 +64,9 @@
         got = lax.ppermute(near_block(shift).astype(NARROW), "fs", perm)
         held = held + got.astype(jnp.float32)
 
+    if ahead is not None:
+        held, ahead = lax.optimization_barrier((held, ahead))
+
     def far_block(shift):
         return lax.dynamic_index_in_dim(held, lax.rem(me // pair + shift, far), 0, keepdims=False)
 
@@ -72,7 +75,7 @@
         perm = [(at, (at + shift * pair) % groups) for at in range(groups)]
         got = lax.ppermute(far_block(shift).astype(NARROW), "fs", perm)
         total = total + got.astype(jnp.float32)
-    return total
+    return total, ahead
 
 
 def exchange(blocks, axis):
@@ -127,12 +130,6 @@
     chunks = CHUNKS if half % (128 * CHUNKS) == 0 else 1
     share = share.reshape(groups, rows, half)
     step = half // chunks
-    share = jnp.concatenate(
-        [fs_sum(share[:, :, at * step : (at + 1) * step]) for at in range(chunks)], axis=1
-    )
-    share = gather_blocks(share, "tp")
-    grad_inputs = share.transpose(1, 0, 2).reshape(rows, width)
-
     def spread(term):
         term = term.reshape(groups, reps, part, mine).transpose(1, 0, 2, 3)
         return exchange(scatter_sum(term, "rep").astype(NARROW), "fs")
@@ -141,8 +138,17 @@
         term = gather_blocks(term, "rep")
         return term.transpose(0, 2, 1, 3).reshape(depth, units).astype(jnp.float32)
 
-    down_turned = whole(spread(contract(cot, hidden, 0, 0)))
-    grad_up = whole(spread(contract(tokens, pre_grad, 0, 0)))
+    spreads = (spread(contract(cot, hidden, 0, 0)), spread(contract(tokens, pre_grad, 0, 0)))
+    sums = []
+    for at in range(chunks):
+        ahead = spreads if at == chunks - 1 else None
+        total, ahead = fs_sum(share[:, :, at * step : (at + 1) * step], ahead)
+        sums.append(total)
+    share = jnp.concatenate(sums, axis=1)
+    share = gather_blocks(share, "tp")
+    grad_inputs = share.transpose(1, 0, 2).reshape(rows, width)
+
+    down_turned, grad_up = whole(ahead[0]), whole(ahead[1])
     norms_up = small_sum(jnp.sum(grad_up * grad_up, axis=1), "tp")
     norms_down = small_sum(jnp.sum(down_turned * down_turned, axis=0), "fs")
     return (grad_inputs, grad_up, down_turned.T, norms_up, norms_down)

time: 351 us -> 343 us (0.977)
  starting transfers between devices: 38.8 us -> 33.4 us
    ppermute x7, waiting for transfers between devices: 44.5 us -> 36.9 us  [rotate(): lax.ppermute(block, axis, [(at, (at + shift) % size) for at in range(size)])]
    ppermute x2, waiting for transfers between devices: 15.6 us -> 22 us  [fs_sum(): got = lax.ppermute(near_block(shift).astype(NARROW), 'fs', perm)]
    ppermute x4, starting transfers between devices: 7.29 us -> 2.31 us  [small_sum(): lax.ppermute(value, axis, [(at, at ^ bit) for at in range(size)])]
    unnamed x38 -> x28, local copies, waits for them, and re-layouts: 14 us -> 10.5 us
  transfers between devices with their start and end apart: 23 -> 23, of which waited for: 10 -> 12; matrix products, arithmetic and copies ran while one was open for 16% -> 16% of each run, Pallas kernels for 0% -> 0%
where the time goes in v3:
time: 343 us; the launch traced here: 342 us
  waiting for transfers between devices  169 us (49%)
  blocking collectives  49.7 us (14%)
  matrix products  33.8 us (10%)
  starting transfers between devices  33.4 us (10%)
  local copies, waits for them, and re-layouts  23.4 us (7%)
  other arithmetic  18.4 us (5%)
  between operations  14.4 us (4%)
    all_gather x1, waiting for transfers between devices, token_plan(): lax.all_gather(own_block(cotangent.reshape(cores, rows // cores, width),...  68.6 us
    all_to_all x1, blocking collectives, exchange(): return lax.all_to_all(blocks, axis, 0, 0)  49.7 us
    ppermute x7, waiting for transfers between devices, rotate(): lax.ppermute(block, axis, [(at, (at + shift) % size) for at in range(size)])  36.9 us
    dot_general x6, matrix products, contract(): lax.dot_general(left, right, (((left_dim,), (right_dim,)), ((), ())), pre...  33.8 us
    ppermute x2, waiting for transfers between devices, fs_sum(): got = lax.ppermute(near_block(shift).astype(NARROW), 'fs', perm)  22 us
    all_gather x1, waiting for transfers between devices, token_plan(): lax.all_gather(own_block(inputs.reshape(cores, rows // cores, width), 'tp...  18.6 us
    ppermute x6, waiting for transfers between devices, fs_sum(): got = lax.ppermute(far_block(shift).astype(NARROW), 'fs', perm)  17.6 us
    ppermute x6, starting transfers between devices, fs_sum(): got = lax.ppermute(far_block(shift).astype(NARROW), 'fs', perm)  10.6 us
  transfers between devices with their start and end apart: 23, of which 12 were waited for; matrix products, arithmetic and copies ran while one was open for 16% of the time, Pallas kernels for 0%

profile of v3, /device:TPU:0, one launch (start us, length us, event | category | flops | bytes accessed | tf_op | source)
XLA Modules:
  0.0 341.9 jit_solution(2736152882394223812)
XLA Ops:
  7.2 1.1 copy-done
  9.3 2.0 constant_dynamic-slice_fusion
  12.4 49.7 %all_to_all.15 = bf16[8,256,256]{2,1,0:T(8,128)(2,1)S(1)} all-to-all(bf16[8,256,256]{2,1,0:T(8,128)(2,1)S(1)} %copy.33), channel_id=1, replica_groups=mesh['rep'=2,'fs'=8,'tp'=2] {'fs'}, dimensions={0} | all-to-all | bytes 2097152 | tf_op jit(solution)/shard_map/all_to_all | solution.py:82
  62.1 1.5 collective-permute-start
  63.6 22.0 %collective-permute-done = bf16[8,256,256]{2,1,0:T(8,128)(2,1)S(1)} collective-permute-done((bf16[8,256,256]{2,1,0:T(8,128)(2,1)S(1)}, bf16[8,256,256]{2,1,0:T(8,128)(2,1)S(1)}, u32[]{:S(2)}, u32[]{:S(2)}) %collective-permute-start) | collective-permute-done | bytes 1048608 | tf_op jit(solution)/shard_map/ppermute | solution.py:25
  86.8 18.6 %all-gather.5.cloned.1.call-done = bf16[1,2048,2048]{2,1,0:T(8,128)(2,1)} async-done(((bf16[1,128,2048]{2,1,0:T(8,128)(2,1)}), bf16[1,2048,2048]{2,1,0:T(8,128)(2,1)}) %all-gather.5.cloned.1.call-update) | async-done | bytes 8388624 | tf_op jit(solution)/shard_map/all_gather | solution.py:112
  105.4 7.1 %fusion.8 = f32[2048,256]{1,0:T(8,128)} fusion(bf16[2048,256]{1,0:T(8,128)(2,1)S(1)} %bitcast.161, bf16[1,2048,2048]{2,1,0:T(8,128)(2,1)} %all-gather.5.cloned.1.call-done), kind=kOutput, calls=%fused_computation.10 | convolution fusion | flops 2148007936 | bytes 11534336 | tf_op jit(solution)/shard_map/dot_general | solution.py:11
  112.5 68.6 %all-gather.7.cloned.1.call-done = bf16[1,2048,2048]{2,1,0:T(8,128)(2,1)} async-done(((bf16[1,128,2048]{2,1,0:T(8,128)(2,1)}), bf16[1,2048,2048]{2,1,0:T(8,128)(2,1)}) %all-gather.7.cloned.1.call-update) | async-done | bytes 8388624 | tf_op jit(solution)/shard_map/all_gather | solution.py:115
  181.0 6.4 %fusion.14 = bf16[2048,256]{1,0:T(8,128)(2,1)S(1)} fusion(bf16[256,2048]{1,0:T(8,128)(2,1)S(1)} %bitcast.174, bf16[1,2048,2048]{2,1,0:T(8,128)(2,1)} %all-gather.7.cloned.1.call-done, f32[2048,256]{1,0:T(8,128)} %fusion.8), kind=kOutput, calls=%fused_computation.16 | convolution fusion | flops 2149056512 | bytes 12582912 | tf_op jit(solution)/shard_map/dot_general | solution.py:11
  187.4 3.3 convolution_convert_fusion
  191.0 6.1 %fusion.4 = f32[2048,256]{1,0:T(8,128)S(1)} fusion(bf16[2048,256]{1,0:T(8,128)(2,1)S(1)} %fusion.14, bf16[1,2048,2048]{2,1,0:T(8,128)(2,1)} %all-gather.5.cloned.1.call-done), kind=kOutput, calls=%fused_computation.4 | convolution fusion | flops 2147483648 | bytes 11534336 | tf_op jit(solution)/shard_map/dot_general | solution.py:11
  197.2 1.5 collective-permute-start.8
  198.7 7.4 %fusion = f32[2048,256]{1,0:T(8,128)} fusion(bf16[1,2048,2048]{2,1,0:T(8,128)(2,1)} %all-gather.7.cloned.1.call-done, f32[2048,256]{1,0:T(8,128)S(1)} %copy-done.10), kind=kOutput, calls=%fused_computation | convolution fusion | flops 2148532224 | bytes 12582912 | tf_op jit(solution)/shard_map/dot_general | solution.py:11
  206.1 5.2 %collective-permute-done.8 = bf16[8,128,256]{2,1,0:T(8,128)(2,1)S(1)} collective-permute-done((bf16[8,128,256]{2,1,0:T(8,128)(2,1)S(1)}, bf16[8,128,256]{2,1,0:T(8,128)(2,1)S(1)}, u32[]{:S(2)}, u32[]{:S(2)}) %collective-permute-start.8) | collective-permute-done | bytes 524320 | tf_op jit(solution)/shard_map/ppermute | solution.py:25
  212.3 4.1 %all-to-all-start.2 = ((bf16[8,128,256]{2,1,0:T(8,128)(2,1)}), bf16[8,128,256]{2,1,0:T(8,128)(2,1)}, u32[]{:S(2)}, u32[]{:S(2)}) async-start(bf16[8,128,256]{2,1,0:T(8,128)(2,1)} %fusion.23), calls=%async_computation.2 | async-start | bytes 1048576 | tf_op jit(solution)/shard_map/all_to_all | solution.py:82
  216.4 3.5 %convert_add_fusion = f32[2048,1024]{1,0:T(8,128)S(1)} fusion(bf16[2048,1024]{1,0:T(8,128)(2,1)} %collective-permute-done.1, bf16[2048,256]{1,0:T(8,128)(2,1)S(1)} %fusion.14, bf16[2,1024,256]{2,1,0:T(8,128)(2,1)S(1)} %bitcast.163, s32[]{:T(128)S(6)} %select_n.111), kind=kOutput, calls=%fused_computation.8 | convolution fusion | flops 1077936128 | bytes 14155780 | tf_op jit(solution)/shard_map/dot_general | solution.py:11
  219.9 1.4 fusion.46
  221.5 1.9 collective-permute-start.2
  224.6 1.5 collective-permute-start.7
  226.3 1.9 collective-permute-start.6
  228.2 9.7 %collective-permute-done.7 = bf16[8,128,256]{2,1,0:T(8,128)(2,1)S(1)} collective-permute-done((bf16[8,128,256]{2,1,0:T(8,128)(2,1)S(1)}, bf16[8,128,256]{2,1,0:T(8,128)(2,1)S(1)}, u32[]{:S(2)}, u32[]{:S(2)}) %collective-permute-start.7) | collective-permute-done | bytes 524320 | tf_op jit(solution)/shard_map/ppermute | solution.py:25
  238.9 5.6 %all-to-all-start.1 = ((bf16[8,128,256]{2,1,0:T(8,128)(2,1)}), bf16[8,128,256]{2,1,0:T(8,128)(2,1)}, u32[]{:S(2)}, u32[]{:S(2)}) async-start(bf16[8,128,256]{2,1,0:T(8,128)(2,1)} %fusion.24), calls=%async_computation.1 | async-start | bytes 1048576 | tf_op jit(solution)/shard_map/all_to_all | solution.py:82
  244.5 6.3 %collective-permute-done.2 = bf16[4,256,512]{2,1,0:T(8,128)(2,1)S(1)} collective-permute-done((bf16[4,256,512]{2,1,0:T(8,128)(2,1)S(1)}, bf16[4,256,512]{2,1,0:T(8,128)(2,1)S(1)}, u32[]{:S(2)}, u32[]{:S(2)}) %collective-permute-start.2) | collective-permute-done | bytes 1048608 | tf_op jit(solution)/shard_map/ppermute | solution.py:64
  250.7 2.1 bitcast_add_fusion.1
  253.9 3.0 collective-permute-start.3
  257.9 1.8 collective-permute-start.4
  259.8 15.8 %collective-permute-done.6 = bf16[4,256,512]{2,1,0:T(8,128)(2,1)} collective-permute-done((bf16[4,256,512]{2,1,0:T(8,128)(2,1)S(1)}, bf16[4,256,512]{2,1,0:T(8,128)(2,1)}, u32[]{:S(2)}, u32[]{:S(2)}) %collective-permute-start.6) | collective-permute-done | bytes 1048608 | tf_op jit(solution)/shard_map/ppermute | solution.py:64
  275.6 1.5 bitcast_add_fusion
  277.9 1.7 collective-permute-start.9
  279.6 2.1 collective-permute-start.11
  282.6 1.5 collective-permute-start.13
  284.6 1.4 fusion.30
  286.1 3.2 collective-permute-done.9
  289.2 2.9 collective-permute-done.11
  292.2 11.5 %collective-permute-done.10 = bf16[256,512]{1,0:T(8,128)(2,1)} collective-permute-done((bf16[256,512]{1,0:T(8,128)(2,1)S(1)}, bf16[256,512]{1,0:T(8,128)(2,1)}, u32[]{:S(2)}, u32[]{:S(2)}) %collective-permute-start.10) | collective-permute-done | bytes 262176 | tf_op jit(solution)/shard_map/ppermute | solution.py:76
  303.7 1.2 fusion.28
  306.0 1.1 select_bitcast_fusion.4
  307.8 1.1 select_bitcast_fusion.6
  309.6 1.5 collective-permute-done.16
  312.2 1.5 convert_bitcast_fusion.1
  313.6 2.3 copy.41
  315.9 3.2 copy.52
  319.1 1.2 copy.40
  320.4 2.2 copy.48
  323.7 3.4 collective-permute-done.18
  327.7 1.4 select_bitcast_fusion
  330.9 1.9 pad_maximum_fusion
  332.8 2.2 copy.47
  (75 shorter events, 18.1 us)
Async XLA Ops:
  7.2 1.2 copy-start
  7.2 4.1 %copy-start.9 = (bf16[2048,256]{1,0:T(8,128)(2,1)S(1)}, bf16[2048,256]{1,0:T(8,128)(2,1)}, u32[]{:S(2)}) copy-start(bf16[2048,256]{1,0:T(8,128)(2,1)} %param.7) | copy-start | bytes 3145732
  7.2 98.2 %all-gather.5.cloned.1.call-start = ((), (), s32[]{:S(2)}) async-start(), calls=%async_computation.3 | async-start | bytes 8912896 | tf_op jit(solution)/shard_map/all_gather | solution.py:112
  9.2 2.4 copy-start.8
  9.3 171.8 %all-gather.7.cloned.1.call-start = ((), (), s32[]{:S(2)}) async-start(), calls=%async_computation.4 | async-start | bytes 8912896 | tf_op jit(solution)/shard_map/all_gather | solution.py:115
  62.1 23.5 %collective-permute-start = (bf16[8,256,256]{2,1,0:T(8,128)(2,1)S(1)}, bf16[8,256,256]{2,1,0:T(8,128)(2,1)S(1)}, u32[]{:S(2)}, u32[]{:S(2)}) collective-permute-start(bf16[8,256,256]{2,1,0:T(8,128)(2,1)S(1)} %all_to_all.15), channel_id=1, source_target_pairs={{0,16},{16,0},{1,17},{17,1},{2,18},{18,2},{3,19},{19,3},{4,20},{20... | collective-permute-start | bytes 3145736 | tf_op jit(solution)/shard_map/ppermute | solution.py:25
  190.7 25.7 %collective-permute-start.1 = (bf16[2048,1024]{1,0:T(8,128)(2,1)}, bf16[2048,1024]{1,0:T(8,128)(2,1)}, u32[]{:S(2)}, u32[]{:S(2)}) collective-permute-start(bf16[2048,1024]{1,0:T(8,128)(2,1)} %convolution_convert_fusion), channel_id=1, source_target_pairs={{0,1},{1,0},{2,3},{3,2},{4,5},{5,4},{6,7},{7,6},{8,9},{9,8},{10,11... | collective-permute-start | bytes 12582920 | tf_op jit(solution)/shard_map/ppermute | solution.py:25
  191.0 7.7 %copy-start.10 = (f32[2048,256]{1,0:T(8,128)S(1)}, f32[2048,256]{1,0:T(8,128)}, u32[]{:S(2)}) copy-start(f32[2048,256]{1,0:T(8,128)} %fusion.8) | copy-start | bytes 6291460
  197.2 14.2 %collective-permute-start.8 = (bf16[8,128,256]{2,1,0:T(8,128)(2,1)S(1)}, bf16[8,128,256]{2,1,0:T(8,128)(2,1)S(1)}, u32[]{:S(2)}, u32[]{:S(2)}) collective-permute-start(bf16[8,128,256]{2,1,0:T(8,128)(2,1)S(1)} %fusion.26), channel_id=1, source_target_pairs={{0,16},{16,0},{1,17},{17,1},{2,18},{18,2},{3,19},{19,3},{4,20},{20... | collective-permute-start | bytes 1572872 | tf_op jit(solution)/shard_map/ppermute | solution.py:25
  212.3 26.6 %all-to-all-start.2 = ((bf16[8,128,256]{2,1,0:T(8,128)(2,1)}), bf16[8,128,256]{2,1,0:T(8,128)(2,1)}, u32[]{:S(2)}, u32[]{:S(2)}) async-start(bf16[8,128,256]{2,1,0:T(8,128)(2,1)} %fusion.23), calls=%async_computation.2 | async-start | bytes 1048576 | tf_op jit(solution)/shard_map/all_to_all | solution.py:82
  221.4 4.9 %copy-start.2 = (f32[8,256,512]{2,1,0:T(8,128)}, f32[8,256,512]{2,1,0:T(8,128)S(1)}, u32[]{:S(2)}) copy-start(f32[8,256,512]{2,1,0:T(8,128)S(1)} %get-tuple-element.12) | copy-start | bytes 12582916
  221.4 6.9 %copy-start.4 = (f32[8,256,512]{2,1,0:T(8,128)}, f32[8,256,512]{2,1,0:T(8,128)S(1)}, u32[]{:S(2)}) copy-start(f32[8,256,512]{2,1,0:T(8,128)S(1)} %get-tuple-element.11) | copy-start | bytes 12582916
  221.4 3.2 copy-start.7
  221.5 29.2 %collective-permute-start.2 = (bf16[4,256,512]{2,1,0:T(8,128)(2,1)S(1)}, bf16[4,256,512]{2,1,0:T(8,128)(2,1)S(1)}, u32[]{:S(2)}, u32[]{:S(2)}) collective-permute-start(bf16[4,256,512]{2,1,0:T(8,128)(2,1)S(1)} %fusion.19), channel_id=1, source_target_pairs={{0,2},{2,0},{4,6},{6,4},{8,10},{10,8},{12,14},{14,12},{1,3},{3,1},... | collective-permute-start | bytes 3145736 | tf_op jit(solution)/shard_map/ppermute | solution.py:64
  224.6 13.3 %collective-permute-start.7 = (bf16[8,128,256]{2,1,0:T(8,128)(2,1)S(1)}, bf16[8,128,256]{2,1,0:T(8,128)(2,1)S(1)}, u32[]{:S(2)}, u32[]{:S(2)}) collective-permute-start(bf16[8,128,256]{2,1,0:T(8,128)(2,1)S(1)} %fusion.25), channel_id=1, source_target_pairs={{0,16},{16,0},{1,17},{17,1},{2,18},{18,2},{3,19},{19,3},{4,20},{20... | collective-permute-start | bytes 1572872 | tf_op jit(solution)/shard_map/ppermute | solution.py:25
  226.3 49.2 %collective-permute-start.6 = (bf16[4,256,512]{2,1,0:T(8,128)(2,1)S(1)}, bf16[4,256,512]{2,1,0:T(8,128)(2,1)}, u32[]{:S(2)}, u32[]{:S(2)}) collective-permute-start(bf16[4,256,512]{2,1,0:T(8,128)(2,1)S(1)} %fusion.20), channel_id=1, source_target_pairs={{0,2},{2,0},{4,6},{6,4},{8,10},{10,8},{12,14},{14,12},{1,3},{3,1},... | collective-permute-start | bytes 3145736 | tf_op jit(solution)/shard_map/ppermute | solution.py:64
  238.9 38.2 %all-to-all-start.1 = ((bf16[8,128,256]{2,1,0:T(8,128)(2,1)}), bf16[8,128,256]{2,1,0:T(8,128)(2,1)}, u32[]{:S(2)}, u32[]{:S(2)}) async-start(bf16[8,128,256]{2,1,0:T(8,128)(2,1)} %fusion.24), calls=%async_computation.1 | async-start | bytes 1048576 | tf_op jit(solution)/shard_map/all_to_all | solution.py:82
  250.7 24.8 %copy-start.3 = (f32[8,256,512]{2,1,0:T(8,128)S(1)}, f32[8,256,512]{2,1,0:T(8,128)}, u32[]{:S(2)}) copy-start(f32[8,256,512]{2,1,0:T(8,128)} %copy-done.2) | copy-start | bytes 12582916
  252.8 6.9 %copy-start.6 = (f32[4,256,512]{2,1,0:T(8,128)}, f32[4,256,512]{2,1,0:T(8,128)S(1)}, u32[]{:S(2)}) copy-start(f32[4,256,512]{2,1,0:T(8,128)S(1)} %bitcast_add_fusion.1) | copy-start | bytes 6291460
  253.9 27.9 %collective-permute-start.3 = (bf16[256,512]{1,0:T(8,128)(2,1)}, bf16[256,512]{1,0:T(8,128)(2,1)}, u32[]{:S(2)}, u32[]{:S(2)}) collective-permute-start(bf16[256,512]{1,0:T(8,128)(2,1)} %get-tuple-element.15), channel_id=1, source_target_pairs={{0,4},{2,6},{4,8},{6,10},{8,12},{10,14},{12,0},{14,2},{1,5},{3,7},... | collective-permute-start | bytes 786440 | tf_op jit(solution)/shard_map/ppermute | solution.py:76
  256.9 25.7 %collective-permute-start.5 = (bf16[256,512]{1,0:T(8,128)(2,1)}, bf16[256,512]{1,0:T(8,128)(2,1)}, u32[]{:S(2)}, u32[]{:S(2)}) collective-permute-start(bf16[256,512]{1,0:T(8,128)(2,1)} %get-tuple-element.16), channel_id=1, source_target_pairs={{0,12},{2,14},{4,0},{6,2},{8,4},{10,6},{12,8},{14,10},{1,13},{3,15... | collective-permute-start | bytes 786440 | tf_op jit(solution)/shard_map/ppermute | solution.py:76
  257.9 26.1 %collective-permute-start.4 = (bf16[256,512]{1,0:T(8,128)(2,1)S(1)}, bf16[256,512]{1,0:T(8,128)(2,1)}, u32[]{:S(2)}, u32[]{:S(2)}) collective-permute-start(bf16[256,512]{1,0:T(8,128)(2,1)S(1)} %get-tuple-element.17), channel_id=1, source_target_pairs={{0,8},{2,10},{4,12},{6,14},{8,0},{10,2},{12,4},{14,6},{1,9},{3,11}... | collective-permute-start | bytes 786440 | tf_op jit(solution)/shard_map/ppermute | solution.py:76
  277.9 11.3 %collective-permute-start.9 = (bf16[256,512]{1,0:T(8,128)(2,1)}, bf16[256,512]{1,0:T(8,128)(2,1)}, u32[]{:S(2)}, u32[]{:S(2)}) collective-permute-start(bf16[256,512]{1,0:T(8,128)(2,1)} %get-tuple-element.18), channel_id=1, source_target_pairs={{0,4},{2,6},{4,8},{6,10},{8,12},{10,14},{12,0},{14,2},{1,5},{3,7},... | collective-permute-start | bytes 786440 | tf_op jit(solution)/shard_map/ppermute | solution.py:76
  279.6 12.6 %collective-permute-start.11 = (bf16[256,512]{1,0:T(8,128)(2,1)S(1)}, bf16[256,512]{1,0:T(8,128)(2,1)}, u32[]{:S(2)}, u32[]{:S(2)}) collective-permute-start(bf16[256,512]{1,0:T(8,128)(2,1)S(1)} %get-tuple-element.19), channel_id=1, source_target_pairs={{0,12},{2,14},{4,0},{6,2},{8,4},{10,6},{12,8},{14,10},{1,13},{3,15... | collective-permute-start | bytes 786440 | tf_op jit(solution)/shard_map/ppermute | solution.py:76
  281.8 21.9 %collective-permute-start.10 = (bf16[256,512]{1,0:T(8,128)(2,1)S(1)}, bf16[256,512]{1,0:T(8,128)(2,1)}, u32[]{:S(2)}, u32[]{:S(2)}) collective-permute-start(bf16[256,512]{1,0:T(8,128)(2,1)S(1)} %get-tuple-element.20), channel_id=1, source_target_pairs={{0,8},{2,10},{4,12},{6,14},{8,0},{10,2},{12,4},{14,6},{1,9},{3,11}... | collective-permute-start | bytes 786440 | tf_op jit(solution)/shard_map/ppermute | solution.py:76
  282.6 25.2 %collective-permute-start.13 = (bf16[8,128,256]{2,1,0:T(8,128)(2,1)}, bf16[8,128,256]{2,1,0:T(8,128)(2,1)S(1)}, u32[]{:S(2)}, u32[]{:S(2)}) collective-permute-start(bf16[8,128,256]{2,1,0:T(8,128)(2,1)} %all-to-all-done.2), channel_id=1, source_target_pairs={{0,16},{16,0},{1,17},{17,1},{2,18},{18,2},{3,19},{19,3},{4,20},{20... | collective-permute-start | bytes 1572872 | tf_op jit(solution)/shard_map/ppermute | solution.py:25
  284.1 22.0 %collective-permute-start.14 = (bf16[8,128,256]{2,1,0:T(8,128)(2,1)}, bf16[8,128,256]{2,1,0:T(8,128)(2,1)S(1)}, u32[]{:S(2)}, u32[]{:S(2)}) collective-permute-start(bf16[8,128,256]{2,1,0:T(8,128)(2,1)} %all-to-all-done.1), channel_id=1, source_target_pairs={{0,16},{16,0},{1,17},{17,1},{2,18},{18,2},{3,19},{19,3},{4,20},{20... | collective-permute-start | bytes 1572872 | tf_op jit(solution)/shard_map/ppermute | solution.py:25
  306.0 21.7 %collective-permute-start.12 = (f32[256,1024]{1,0:T(8,128)}, f32[256,1024]{1,0:T(8,128)}, u32[]{:S(2)}, u32[]{:S(2)}) collective-permute-start(f32[256,1024]{1,0:T(8,128)} %pad_maximum_fusion.3), channel_id=1, source_target_pairs={{0,1},{1,0},{2,3},{3,2},{4,5},{5,4},{6,7},{7,6},{8,9},{9,8},{10,11... | collective-permute-start | bytes 3145736 | tf_op jit(solution)/shard_map/ppermute | solution.py:25
  307.4 3.7 %collective-permute-start.16 = (f32[2048]{0:T(1024)S(1)}, f32[2048]{0:T(1024)S(1)}, u32[]{:S(2)}, u32[]{:S(2)}) collective-permute-start(f32[2048]{0:T(1024)S(1)} %bitcast.178), channel_id=1, source_target_pairs={{0,2},{2,0},{4,6},{6,4},{8,10},{10,8},{12,14},{14,12},{1,3},{3,1},... | collective-permute-start | bytes 24584 | tf_op jit(solution)/shard_map/ppermute | solution.py:91
  309.2 14.0 %collective-permute-start.15 = (f32[256]{0:T(256)S(1)}, f32[256]{0:T(256)S(1)}, u32[]{:S(2)}, u32[]{:S(2)}) collective-permute-start(f32[256]{0:T(256)S(1)} %bitcast.180), channel_id=1, source_target_pairs={{0,1},{1,0},{2,3},{3,2},{4,5},{5,4},{6,7},{7,6},{8,9},{9,8},{10,11... | collective-permute-start | bytes 3080 | tf_op jit(solution)/shard_map/ppermute | solution.py:91
  311.1 11.4 %collective-permute-start.17 = (f32[2048]{0:T(1024)S(1)}, f32[2048]{0:T(1024)S(1)}, u32[]{:S(2)}, u32[]{:S(2)}) collective-permute-start(f32[2048]{0:T(1024)S(1)} %add.165), channel_id=1, source_target_pairs={{0,4},{2,6},{4,0},{6,2},{8,12},{10,14},{12,8},{14,10},{1,5},{3,7},... | collective-permute-start | bytes 24584 | tf_op jit(solution)/shard_map/ppermute | solution.py:91
  315.9 3.2 copy-start.5
  322.6 4.6 %collective-permute-start.18 = (f32[2048]{0:T(1024)S(1)}, f32[2048]{0:T(1024)S(1)}, u32[]{:S(2)}, u32[]{:S(2)}) collective-permute-start(f32[2048]{0:T(1024)S(1)} %add.166), channel_id=1, source_target_pairs={{0,8},{2,10},{4,12},{6,14},{8,0},{10,2},{12,4},{14,6},{1,9},{3,11}... | collective-permute-start | bytes 24584 | tf_op jit(solution)/shard_map/ppermute | solution.py:91
  332.8 2.2 copy-start.1
Sparse Core Ops, SparseCore 0:
  10.7 94.6 all-gather.4
  108.1 72.8 all-gather.6
